TPU v7x, 128 devices: a whole 4x4x4 slice. The times are simulated.
128 devices in a mesh: sp: 64 (over z, y, x), tp: 2 (over core).
Axes of the slice: x: 4, y: 4, z: 4, core: 2. Of those that a mesh axis runs over, the one named last changes fastest.
Arguments:
- residual: bfloat16 [16384, 2048], P(('sp', 'tp')), may hold values from -6 to 6
- queries: bfloat16 [16384, 512], P('sp', 'tp'), may hold values from -6 to 6
- key_rows: bfloat16 [16384, 512], P('sp', 'tp'), may hold values from -6 to 6
- value_rows: bfloat16 [16384, 1024], P('sp', 'tp'), may hold values from -6 to 6
- out_gate: bfloat16 [16384, 1024], P('sp', 'tp'), may hold values from -6 to 6
- gate_logits: bfloat16 [16384, 512], P('sp', 'tp')
- head_gain: float32 [128], replicated, may hold values from 0.1 to 1.9
- out_weight: bfloat16 [1024, 2048], replicated, may hold values from -0.1875 to 0.1875
- norm_gain: float32 [2048], replicated, may hold values from 0.1 to 1.9
- routes: int32 [16384, 2], P(('sp', 'tp')), may hold values from 0 to 127, as said below
- group_score: float32 [16384], P(('sp', 'tp')), may hold values from 0.25 to 1
- expert_score: float32 [16384, 2], P(('sp', 'tp')), may hold values from 0.1 to 1
- gate_weight: bfloat16 [128, 2048, 512], P(('sp', 'tp')), may hold values from -0.125 to 0.125
- up_weight: bfloat16 [128, 2048, 512], P(('sp', 'tp')), may hold values from -0.125 to 0.125
- down_weight: bfloat16 [128, 512, 2048], P(('sp', 'tp')), may hold values from -0.25 to 0.25
Outputs:
- layer_out: bfloat16 [16384, 2048], P(('sp', 'tp'))
Inputs may be any that keep to these rules, and one draw needn't show every extreme that they name: `routes`: the two experts of a token differ and lie in one group of 8 consecutive expert numbers. In each aligned block of 128 tokens (the tokens of one device) no expert is named more than 3 times, and one expert, the same for all blocks of a draw, is named exactly 3 times in every block.
All inputs are finite; a program needn't handle non-finite values.
Results may differ from a plain program's by a relative error of at most 0.0056.
Values may be sent and summed in bfloat16 or wider, within the bound.
A program may use at most 64 MiB of HBM per device.

v0:
```python
import jax
import jax.numpy as jnp
from jax import lax
from jax.sharding import Mesh
from jax.sharding import PartitionSpec as P

KEY_DIM = 64
VALUE_DIM = 128
BLOCK = 64
SP = ("sp_0", "sp_1", "sp_2")
SP_TP = ("sp_0", "sp_1", "sp_2", "tp")


def neutral_like(value, identity):
    return jax.tree.map(
        lambda part, zero: jnp.zeros_like(part) + jnp.asarray(zero, part.dtype), value, identity
    )


def entering_2(value, axes, combine, identity):
    before = start = neutral_like(value, identity)
    so_far = value
    for axis in reversed(axes):
        peers, place = (lax.axis_size(axis), lax.axis_index(axis))
        pieces = jax.tree.map(lambda part: lax.all_gather(part, axis), so_far)
        inside, so_far = (start, start)
        for k in range(peers):
            passed = k < place
            so_far = combine(so_far, jax.tree.map(lambda part: part[k], pieces))
            inside = jax.tree.map(lambda new, old: jnp.where(passed, new, old), so_far, inside)
        before = combine(inside, before)
    return before


def block_parts(queries, key_rows, value_rows, gate_logits):
    length = queries.shape[0]
    head_count = queries.shape[1] // KEY_DIM
    blocks = length // BLOCK

    def arrange(source, inner_size):
        return (
            source.astype(jnp.float32)
            .reshape(blocks, BLOCK, head_count, inner_size)
            .transpose(0, 2, 1, 3)
        )

    decay_log = jax.nn.log_sigmoid(gate_logits.astype(jnp.float32)) / 16.0
    running = jnp.cumsum(arrange(decay_log, KEY_DIM), axis=2)
    closing = running[:, :, -1:, :]
    query_scaled = arrange(queries, KEY_DIM) * KEY_DIM ** (-0.5) * jnp.exp(running)
    key_float = arrange(key_rows, KEY_DIM)
    key_inverse = key_float * jnp.exp(-running)
    key_closing = key_float * jnp.exp(closing - running)
    value_float = arrange(value_rows, VALUE_DIM)
    causal = jnp.tril(jnp.ones((BLOCK, BLOCK), dtype=bool))
    scores = jnp.where(
        causal,
        jnp.einsum("nhcd,nhsd->nhcs", query_scaled, key_inverse, precision=lax.Precision.HIGHEST),
        0.0,
    )
    within = jnp.einsum("nhcs,nhsv->nhcv", scores, value_float, precision=lax.Precision.HIGHEST)
    increments = jnp.einsum(
        "nhcd,nhcv->nhdv", key_closing, value_float, precision=lax.Precision.HIGHEST
    )
    return (query_scaled, within, increments, closing[:, :, 0, :])


def advance(carried, inputs):
    increment, block_log = inputs
    return (jnp.exp(block_log)[..., None] * carried + increment, carried)


def finish(attended, head_gain, out_gate):
    blocks = attended.shape[0]
    head_count = attended.shape[1]
    length = blocks * BLOCK
    ordered = attended.transpose(0, 2, 1, 3).reshape(length, head_count, VALUE_DIM)
    normed = (
        ordered * lax.rsqrt(jnp.mean(ordered * ordered, axis=-1, keepdims=True) + 1e-06) * head_gain
    )
    gating = jax.nn.silu(out_gate.astype(jnp.float32)).reshape(length, head_count, VALUE_DIM)
    return (normed * gating).reshape(length, head_count * VALUE_DIM).astype(jnp.bfloat16)


def route_slots(block_routes, experts_total, capacity):
    row_count = block_routes.shape[0]
    flattened = block_routes.reshape(-1)
    onehot = (flattened[:, None] == jnp.arange(experts_total, dtype=jnp.int32)[None, :]).astype(
        jnp.int32
    )
    ranking = jnp.sum((jnp.cumsum(onehot, axis=0) - onehot) * onehot, axis=1)
    slot_index = flattened * capacity + ranking
    route_ids = jnp.arange(2 * row_count, dtype=jnp.int32) // 2
    owners = (
        jnp.full((experts_total * capacity,), row_count, jnp.int32).at[slot_index].set(route_ids)
    )
    return (slot_index, owners)


def expert_apply(rows_in, gate_matrix, up_matrix, down_matrix):
    gated = jnp.dot(rows_in, gate_matrix, preferred_element_type=jnp.float32)
    lifted = jnp.dot(rows_in, up_matrix, preferred_element_type=jnp.float32)
    inner_rows = (jax.nn.silu(gated) * lifted).astype(jnp.bfloat16)
    return jnp.dot(inner_rows, down_matrix, preferred_element_type=jnp.float32).astype(jnp.bfloat16)


def merge_states(earlier, later):
    return (earlier[0] * later[0], later[0][..., None] * earlier[1] + later[1])


def local(
    residual,
    queries,
    key_rows,
    value_rows,
    out_gate,
    gate_logits,
    head_gain,
    out_weight,
    norm_gain,
    routes,
    group_score,
    expert_score,
    gate_weight,
    up_weight,
    down_weight,
):
    query_scaled, within, increments, block_logs = block_parts(
        queries, key_rows, value_rows, gate_logits
    )
    zero_state = jnp.zeros(increments.shape[1:], jnp.float32)
    local_end, local_prefix = lax.scan(advance, zero_state, (increments, block_logs))
    device_decay = jnp.exp(jnp.sum(block_logs, axis=0))
    identity = (jnp.ones_like(device_decay), jnp.zeros_like(local_end))
    entering = entering_2((device_decay, local_end), SP, merge_states, identity)[1]
    leading = jnp.exp(jnp.cumsum(block_logs, axis=0) - block_logs)
    states = leading[..., None] * entering[None] + local_prefix
    attended = within + jnp.einsum(
        "nhcd,nhdv->nhcv", query_scaled, states, precision=lax.Precision.HIGHEST
    )
    mixer_out = finish(attended, head_gain, out_gate)
    row_count = residual.shape[0]
    model_width = residual.shape[1]
    pair_count = lax.axis_size("tp")
    chip_count = lax.axis_size(SP)
    regrouped = lax.all_to_all(mixer_out, "tp", split_axis=0, concat_axis=1, tiled=True)
    projected = jnp.dot(regrouped, out_weight, preferred_element_type=jnp.float32)
    merged = (residual.astype(jnp.float32) + projected).astype(jnp.bfloat16)
    widened = lax.optimization_barrier(merged).astype(jnp.float32)
    normed = (
        widened * lax.rsqrt(jnp.mean(widened * widened, axis=-1, keepdims=True) + 1e-06) * norm_gain
    ).astype(jnp.bfloat16)
    experts_total = chip_count * pair_count
    capacity = 3 * row_count // experts_total
    slot_index, owners = route_slots(routes, experts_total, capacity)
    padded = jnp.concatenate([normed, jnp.zeros((1, model_width), jnp.bfloat16)], axis=0)
    outgoing = padded[owners].reshape(experts_total, capacity, model_width)
    gate_matrix = gate_weight[0]
    up_matrix = up_weight[0]
    down_matrix = down_weight[0]
    arrived = lax.all_to_all(outgoing, SP_TP, split_axis=0, concat_axis=0, tiled=True)
    shape_in = arrived.shape
    served = expert_apply(arrived.reshape(-1, shape_in[-1]), gate_matrix, up_matrix, down_matrix)
    returned = lax.all_to_all(
        served.reshape(shape_in), SP_TP, split_axis=0, concat_axis=0, tiled=True
    )
    picked = returned.reshape(experts_total * capacity, model_width)[slot_index].reshape(
        row_count, 2, model_width
    )
    weights = group_score[:, None] * expert_score / jnp.sum(expert_score, axis=1, keepdims=True)
    combined = weights[:, 0:1] * picked[:, 0].astype(jnp.float32) + weights[:, 1:2] * picked[
        :, 1
    ].astype(jnp.float32)
    return (widened + combined).astype(jnp.bfloat16)


def solution(mesh):
    torus = Mesh(mesh.devices.reshape(4, 4, 4, mesh.shape["tp"]), ("sp_0", "sp_1", "sp_2", "tp"))
    in_specs = (
        P(SP_TP, None),
        P(SP, "tp"),
        P(SP, "tp"),
        P(SP, "tp"),
        P(SP, "tp"),
        P(SP, "tp"),
        P(),
        P(),
        P(),
        P(SP_TP, None),
        P(SP_TP),
        P(SP_TP, None),
        P(SP_TP, None, None),
        P(SP_TP, None, None),
        P(SP_TP, None, None),
    )
    out_specs = P(SP_TP, None)
    return jax.shard_map(local, mesh=torus, in_specs=in_specs, out_specs=out_specs, check_vma=False)
```

profile of v0, /device:TPU:1, one launch (start us, length us, event | category | flops | bytes accessed | tf_op | source)
XLA Modules:
  0.0 230.2 jit_solution(4951498174471461953)
XLA Ops:
  0.0 1.3 fusion.43
  2.1 9.3 %all-gather.2 = f32[4,4,64]{2,1,0:T(4,128)S(1)} all-gather(f32[1,4,64]{2,1,0:T(4,128)S(1)} %exponential_bitcast_fusion.1), channel_id=2, replica_groups=mesh['sp_0'=4,'sp_1'=4,'sp_2'=4,'tp'=2] {'sp_2'}, dimensions={0}, use_global_device_ids=true | all-gather | bytes 5120 | tf_op jit(solution)/shard_map/all_gather | solution.py:25
  12.6 9.0 %all_gather.27 = f32[4,4,64]{2,1,0:T(4,128)} all-gather(f32[1,4,64]{2,1,0:T(4,128)S(1)} %multiply_bitcast_fusion), channel_id=1, replica_groups=mesh['sp_0'=4,'sp_1'=4,'sp_2'=4,'tp'=2] {'sp_1'}, dimensions={0}, use_global_device_ids=true | all-gather | bytes 5120 | tf_op jit(solution)/shard_map/all_gather | solution.py:25
  21.9 1.0 reshape.228
  22.9 0.6 fusion.13
  23.5 1.4 fusion.31
  24.9 6.9 %while.13 = (s32[]{:T(128)}, f32[4,64,128]{2,1,0:T(8,128)S(1)}, f32[4,4,64,128]{3,2,1,0:T(8,128)}, f32[4,4,64]{2,1,0:T(4,128)S(1)}, f32[4,4,64,128]{3,2,1,0:T(8,128)}, /*index=5*/s32[]{:T(128)}, s32[]{:T(128)}) while((s32[]{:T(128)}, f32[4,64,128]{2,1,0:T(8,128)S(1)}, f32[4,4,64,128]{3,2,1,0:T(8,128)}, f32[4,4,64]{2,1,0:T(4,128)S(1)}, ...), condition=%wide.region_4.5_spmd.clone, body=%wide.region_3.4_spmd.clone.sunk | while | flops 131075 | bytes 659040 | solution.py:132
  24.9 0.7 bitcast_dynamic-update-slice_fusion.2
  25.6 1.0 bitcast_add_fusion.2
  26.6 0.7 bitcast_dynamic-update-slice_fusion.2
  27.3 1.0 bitcast_add_fusion.2
  28.4 0.7 bitcast_dynamic-update-slice_fusion.2
  29.0 1.0 bitcast_add_fusion.2
  30.1 0.7 bitcast_dynamic-update-slice_fusion.2
  30.7 1.0 bitcast_add_fusion.2
  31.8 10.0 %all-gather.1 = f32[16,64,128]{2,1,0:T(8,128)S(1)} all-gather(f32[4,64,128]{2,1,0:T(8,128)S(1)} %get-tuple-element.33), channel_id=3, replica_groups=mesh['sp_0'=4,'sp_1'=4,'sp_2'=4,'tp'=2] {'sp_2'}, dimensions={0}, use_global_device_ids=true | all-gather | bytes 655360 | tf_op jit(solution)/shard_map/all_gather | solution.py:25
  41.8 0.7 multiply_multiply_fusion
  42.6 1.3 fusion.69
  43.9 0.9 fusion.57
  44.8 10.2 %all_gather.31 = f32[4,4,64,128]{3,2,1,0:T(8,128)S(1)} all-gather(f32[1,4,64,128]{3,2,1,0:T(8,128)S(1)} %fusion.57), channel_id=1, replica_groups=mesh['sp_0'=4,'sp_1'=4,'sp_2'=4,'tp'=2] {'sp_1'}, dimensions={0}, use_global_device_ids=true | all-gather | bytes 655360 | tf_op jit(solution)/shard_map/all_gather | solution.py:25
  55.0 0.8 copy-done.6
  56.0 12.0 %all_gather.32 = f32[4,4,64,128]{3,2,1,0:T(8,128)} all-gather(f32[1,4,64,128]{3,2,1,0:T(8,128)S(1)} %slice_add_fusion.4), channel_id=1, replica_groups=mesh['sp_0'=4,'sp_1'=4,'sp_2'=4,'tp'=2] {'sp_0'}, dimensions={0}, use_global_device_ids=true | all-gather | bytes 655360 | tf_op jit(solution)/shard_map/all_gather | solution.py:25
  68.0 8.5 %all_gather.28 = f32[4,4,64]{2,1,0:T(4,128)S(1)} all-gather(f32[1,4,64]{2,1,0:T(4,128)S(1)} %get-tuple-element.73), channel_id=1, replica_groups=mesh['sp_0'=4,'sp_1'=4,'sp_2'=4,'tp'=2] {'sp_0'}, dimensions={0}, use_global_device_ids=true | all-gather | bytes 5120 | tf_op jit(solution)/shard_map/all_gather | solution.py:25
  77.2 0.7 convert_multiply_fusion.5
  77.9 2.0 mul.372
  80.0 2.2 convolution_select_fusion
  83.4 1.5 multiply_reduce_fusion
  85.1 1.4 copy.52
  86.9 1.1 fusion.38
  88.1 0.8 copy.55
  88.9 19.7 %all-to-all-start = ((bf16[2,128,512]{1,2,0:T(8,128)(2,1)}), bf16[2,128,512]{1,2,0:T(8,128)(2,1)S(1)}, u32[]{:S(2)}, u32[]{:S(2)}) async-start(bf16[2,128,512]{1,2,0:T(8,128)(2,1)} %copy.55), calls=%async_computation | async-start | bytes 524288 | tf_op jit(solution)/shard_map/all_to_all | solution.py:146
  109.1 0.8 all-to-all-done
  109.9 2.9 %fusion = bf16[128,2048]{1,0:T(8,128)(2,1)S(1)} fusion(bf16[128,1024]{0,1:T(8,128)(2,1)S(1)} %bitcast.224, bf16[1024,2048]{1,0:T(8,128)(2,1)} %param.24, bf16[128,2048]{1,0:T(8,128)(2,1)S(1)} %copy-done.10), kind=kOutput, calls=%fused_computation.8 | convolution fusion | flops 537657344 | bytes 5505024 | tf_op jit(solution)/shard_map/dot_general | solution.py:147
  113.9 1.4 scatter_custom_fusion
  115.6 3.1 %gather_fusion = bf16[384,2048]{1,0:T(8,128)(2,1)} fusion(bf16[129,2048]{1,0:T(8,128)(2,1)S(1)} %concatenate.3, s32[1024]{0:T(1024)S(1)} %pad_clamp_fusion.1), kind=kCustom, calls=%fused_computation | custom fusion | bytes 3147264 | tf_op jit(solution)/shard_map/gather | solution.py:157
  118.7 5.1 %reshape.231 = bf16[128,3,2048]{2,1,0:T(4,128)(2,1)} reshape(bf16[384,2048]{1,0:T(8,128)(2,1)} %gather_fusion) | data formatting | bytes 3145728 | tf_op jit(solution)/shard_map/reshape | solution.py:157
  123.8 36.9 %all_to_all.29 = bf16[128,3,2048]{2,1,0:T(4,128)(2,1)} all-to-all(bf16[128,3,2048]{2,1,0:T(4,128)(2,1)} %reshape.231), channel_id=1, replica_groups=mesh['sp_0'=4,'sp_1'=4,'sp_2'=4,'tp'=2] {'sp_0','sp_1','sp_2','tp'}, dimensions={0} | all-to-all | bytes 3145728 | tf_op jit(solution)/shard_map/all_to_all | solution.py:161
  160.8 5.0 %reshape.232 = bf16[384,2048]{1,0:T(8,128)(2,1)} reshape(bf16[128,3,2048]{2,1,0:T(4,128)(2,1)} %all_to_all.29) | data formatting | bytes 3145728 | tf_op jit(solution)/shard_map/reshape | solution.py:163
  165.8 3.0 %fusion.4 = f32[384,512]{1,0:T(8,128)S(1)} fusion(bf16[384,2048]{1,0:T(8,128)(2,1)} %reshape.232, bf16[1,2048,512]{2,1,0:T(8,128)(2,1)} %param.29), kind=kOutput, calls=%fused_computation.12 | convolution fusion | flops 805306368 | bytes 4456448 | tf_op jit(solution)/shard_map/dot_general | solution.py:101
  168.9 5.2 %convolution_convert_fusion = bf16[384,2048]{1,0:T(8,128)(2,1)} fusion(bf16[1,512,2048]{2,1,0:T(8,128)(2,1)S(1)} %copy-done, bf16[384,2048]{1,0:T(8,128)(2,1)} %reshape.232, bf16[1,2048,512]{2,1,0:T(8,128)(2,1)} %param.30, f32[384,512]{1,0:T(8,128)S(1)} %fusion.4), kind=kOutput, calls=%fused_computation.6 | convolution fusion | flops 1612578816 | bytes 8126464 | tf_op jit(solution)/shard_map/dot_general | solution.py:104
  174.1 5.1 %reshape.233 = bf16[128,3,2048]{2,1,0:T(4,128)(2,1)} reshape(bf16[384,2048]{1,0:T(8,128)(2,1)} %convolution_convert_fusion) | data formatting | bytes 3145728 | tf_op jit(solution)/shard_map/reshape | solution.py:165
  179.2 5.6 %all-to-all-start.2 = ((bf16[128,3,2048]{2,1,0:T(4,128)(2,1)}), bf16[128,3,2048]{2,1,0:T(4,128)(2,1)}, u32[]{:S(2)}, u32[]{:S(2)}) async-start(bf16[128,3,2048]{2,1,0:T(4,128)(2,1)} %reshape.233), calls=%async_computation.2 | async-start | bytes 4194304 | tf_op jit(solution)/shard_map/all_to_all | solution.py:164
  184.9 30.2 %all-to-all-done.2 = bf16[128,3,2048]{2,1,0:T(4,128)(2,1)} async-done(((bf16[128,3,2048]{2,1,0:T(4,128)(2,1)}), bf16[128,3,2048]{2,1,0:T(4,128)(2,1)}, u32[]{:S(2)}, u32[]{:S(2)}) %all-to-all-start.2) | async-done | bytes 1572896 | tf_op jit(solution)/shard_map/all_to_all | solution.py:164
  215.1 5.0 %reshape.234 = bf16[384,2048]{1,0:T(8,128)(2,1)} reshape(bf16[128,3,2048]{2,1,0:T(4,128)(2,1)} %all-to-all-done.2) | data formatting | bytes 3145728 | tf_op jit(solution)/shard_map/reshape | solution.py:167
  220.1 5.0 %gather_fusion.1 = bf16[256,2048]{1,0:T(8,128)(2,1)} fusion(bf16[384,2048]{1,0:T(8,128)(2,1)} %reshape.234, s32[1024]{0:T(1024)S(1)} %pad_clamp_fusion), kind=kCustom, calls=%fused_computation.1 | custom fusion | bytes 2098176 | tf_op jit(solution)/shard_map/gather | solution.py:167
  225.1 1.7 reshape.235
  226.8 1.5 fusion.75
  228.3 1.9 fusion.17
  (123 shorter events, 6.4 us)
Async XLA Ops:
  0.0 168.9 %copy-start = (bf16[1,512,2048]{2,1,0:T(8,128)(2,1)S(1)}, bf16[1,512,2048]{2,1,0:T(8,128)(2,1)}, u32[]{:S(2)}) copy-start(bf16[1,512,2048]{2,1,0:T(8,128)(2,1)} %param.31) | copy-start | bytes 6291460
  0.0 21.6 %copy-start.11 = (bf16[256,256]{1,0:T(8,128)(2,1)S(1)}, bf16[256,256]{1,0:T(8,128)(2,1)}, u32[]{:S(2)}) copy-start(bf16[256,256]{1,0:T(8,128)(2,1)} %param.19) | copy-start | bytes 393220
  31.8 45.4 %copy-start.12 = (bf16[256,256]{1,0:T(8,128)(2,1)S(1)}, bf16[256,256]{1,0:T(8,128)(2,1)}, u32[]{:S(2)}) copy-start(bf16[256,256]{1,0:T(8,128)(2,1)} %param.18) | copy-start | bytes 393220
  41.8 2.1 copy-start.4
  41.8 38.1 %copy-start.14 = (pred[64,64]{1,0:T(8,128)(4,1)S(1)}, pred[64,64]{1,0:T(8,128)(4,1)}, u32[]{:S(2)}) copy-start(pred[64,64]{1,0:T(8,128)(4,1)} %iota_compare_fusion.1) | copy-start | bytes 12292
  42.5 34.6 %copy-start.22 = (f32[4,64]{1,0:T(4,128)}, f32[4,64]{1,0:T(4,128)S(1)}, u32[]{:S(2)}) copy-start(f32[4,64]{1,0:T(4,128)S(1)} %get-tuple-element.74) | copy-start | bytes 3076
  42.5 34.6 %copy-start.24 = (f32[4,64]{1,0:T(4,128)}, f32[4,64]{1,0:T(4,128)S(1)}, u32[]{:S(2)}) copy-start(f32[4,64]{1,0:T(4,128)S(1)} %get-tuple-element.75) | copy-start | bytes 3076
  42.6 34.6 %copy-start.26 = (f32[4,64]{1,0:T(4,128)}, f32[4,64]{1,0:T(4,128)S(1)}, u32[]{:S(2)}) copy-start(f32[4,64]{1,0:T(4,128)S(1)} %get-tuple-element.76) | copy-start | bytes 3076
  43.9 33.3 %copy-start.15 = (f32[4,64]{1,0:T(4,128)}, f32[4,64]{1,0:T(4,128)S(1)}, u32[]{:S(2)}) copy-start(f32[4,64]{1,0:T(4,128)S(1)} %get-tuple-element.77) | copy-start | bytes 3076
  43.9 33.3 %copy-start.17 = (f32[4,64]{1,0:T(4,128)}, f32[4,64]{1,0:T(4,128)S(1)}, u32[]{:S(2)}) copy-start(f32[4,64]{1,0:T(4,128)S(1)} %get-tuple-element.78) | copy-start | bytes 3076
  55.0 0.8 copy-start.6
  79.9 2.8 %copy-start.5 = (f32[16,64,128]{2,1,0:T(8,128)S(1)}, f32[16,64,128]{2,1,0:T(8,128)}, u32[]{:S(2)}) copy-start(f32[16,64,128]{2,1,0:T(8,128)} %copy-done.4) | copy-start | bytes 1572868
  79.9 2.8 %copy-start.7 = (f32[4,4,64,128]{3,2,1,0:T(8,128)S(1)}, f32[4,4,64,128]{3,2,1,0:T(8,128)}, u32[]{:S(2)}) copy-start(f32[4,4,64,128]{3,2,1,0:T(8,128)} %copy-done.6) | copy-start | bytes 1572868
  79.9 2.8 %copy-start.8 = (f32[4,4,64,128]{3,2,1,0:T(8,128)S(1)}, f32[4,4,64,128]{3,2,1,0:T(8,128)}, u32[]{:S(2)}) copy-start(f32[4,4,64,128]{3,2,1,0:T(8,128)} %all_gather.32) | copy-start | bytes 1572868
  79.9 2.8 %copy-start.16 = (f32[4,64]{1,0:T(4,128)S(1)}, f32[4,64]{1,0:T(4,128)}, u32[]{:S(2)}) copy-start(f32[4,64]{1,0:T(4,128)} %copy-done.15) | copy-start | bytes 3076
  79.9 2.8 %copy-start.18 = (f32[4,64]{1,0:T(4,128)S(1)}, f32[4,64]{1,0:T(4,128)}, u32[]{:S(2)}) copy-start(f32[4,64]{1,0:T(4,128)} %copy-done.17) | copy-start | bytes 3076
  79.9 2.8 %copy-start.19 = (f32[4,64]{1,0:T(4,128)S(1)}, f32[4,64]{1,0:T(4,128)}, u32[]{:S(2)}) copy-start(f32[4,64]{1,0:T(4,128)} %get-tuple-element.79) | copy-start | bytes 3076
  79.9 2.8 %copy-start.20 = (f32[4,64]{1,0:T(4,128)S(1)}, f32[4,64]{1,0:T(4,128)}, u32[]{:S(2)}) copy-start(f32[4,64]{1,0:T(4,128)} %get-tuple-element.80) | copy-start | bytes 3076
  79.9 2.8 %copy-start.21 = (f32[4,64]{1,0:T(4,128)S(1)}, f32[4,64]{1,0:T(4,128)}, u32[]{:S(2)}) copy-start(f32[4,64]{1,0:T(4,128)} %get-tuple-element.81) | copy-start | bytes 3076
  79.9 2.8 %copy-start.23 = (f32[4,64]{1,0:T(4,128)S(1)}, f32[4,64]{1,0:T(4,128)}, u32[]{:S(2)}) copy-start(f32[4,64]{1,0:T(4,128)} %copy-done.22) | copy-start | bytes 3076
  79.9 2.8 %copy-start.25 = (f32[4,64]{1,0:T(4,128)S(1)}, f32[4,64]{1,0:T(4,128)}, u32[]{:S(2)}) copy-start(f32[4,64]{1,0:T(4,128)} %copy-done.24) | copy-start | bytes 3076
  80.0 2.8 %copy-start.27 = (f32[4,64]{1,0:T(4,128)S(1)}, f32[4,64]{1,0:T(4,128)}, u32[]{:S(2)}) copy-start(f32[4,64]{1,0:T(4,128)} %copy-done.26) | copy-start | bytes 3076
  80.0 2.8 %copy-start.29 = (f32[4,64]{1,0:T(4,128)S(1)}, f32[4,64]{1,0:T(4,128)}, u32[]{:S(2)}) copy-start(f32[4,64]{1,0:T(4,128)} %get-tuple-element.63) | copy-start | bytes 3076
  80.0 2.8 %copy-start.30 = (f32[4,64]{1,0:T(4,128)S(1)}, f32[4,64]{1,0:T(4,128)}, u32[]{:S(2)}) copy-start(f32[4,64]{1,0:T(4,128)} %get-tuple-element.64) | copy-start | bytes 3076
  80.0 2.8 %copy-start.31 = (f32[4,64]{1,0:T(4,128)S(1)}, f32[4,64]{1,0:T(4,128)}, u32[]{:S(2)}) copy-start(f32[4,64]{1,0:T(4,128)} %get-tuple-element.71) | copy-start | bytes 3076
  80.0 2.8 %copy-start.32 = (f32[4,64]{1,0:T(4,128)S(1)}, f32[4,64]{1,0:T(4,128)}, u32[]{:S(2)}) copy-start(f32[4,64]{1,0:T(4,128)} %get-tuple-element.72) | copy-start | bytes 3076
  82.2 1.2 copy-start.3
  82.2 1.2 copy-start.9
  82.2 1.2 copy-start.13
  83.4 3.2 %copy-start.35 = (f32[128]{0:T(128)S(1)}, f32[128]{0:T(128)}, u32[]{:S(2)}) copy-start(f32[128]{0:T(128)} %param.23) | copy-start | bytes 1540
  85.1 23.6 %copy-start.33 = (s32[128,2]{0,1:T(2,128)S(1)}, s32[128,2]{0,1:T(2,128)}, u32[]{:S(2)}) copy-start(s32[128,2]{0,1:T(2,128)} %param.26) | copy-start | bytes 3076
  85.1 24.7 %copy-start.10 = (bf16[128,2048]{1,0:T(8,128)(2,1)S(1)}, bf16[128,2048]{1,0:T(8,128)(2,1)}, u32[]{:S(2)}) copy-start(bf16[128,2048]{1,0:T(8,128)(2,1)} %param.17) | copy-start | bytes 1572868
  88.9 20.9 %all-to-all-start = ((bf16[2,128,512]{1,2,0:T(8,128)(2,1)}), bf16[2,128,512]{1,2,0:T(8,128)(2,1)S(1)}, u32[]{:S(2)}, u32[]{:S(2)}) async-start(bf16[2,128,512]{1,2,0:T(8,128)(2,1)} %copy.55), calls=%async_computation | async-start | bytes 524288 | tf_op jit(solution)/shard_map/all_to_all | solution.py:146
  109.9 5.5 %copy-start.28 = (f32[2048]{0:T(1024)S(1)}, f32[2048]{0:T(1024)}, u32[]{:S(2)}) copy-start(f32[2048]{0:T(1024)} %param.25) | copy-start | bytes 24580
  112.8 2.5 %copy-start.1 = (bf16[128,2048]{1,0:T(8,128)(2,1)}, bf16[128,2048]{1,0:T(8,128)(2,1)S(1)}, u32[]{:S(2)}) copy-start(bf16[128,2048]{1,0:T(8,128)(2,1)S(1)} %fusion) | copy-start | bytes 1572868
  179.2 5.6 %copy-start.34 = (f32[128,2]{0,1:T(2,128)S(1)}, f32[128,2]{0,1:T(2,128)}, u32[]{:S(2)}) copy-start(f32[128,2]{0,1:T(2,128)} %param.28) | copy-start | bytes 3076
  179.2 5.7 %copy-start.36 = (f32[128]{0:T(128)S(1)}, f32[128]{0:T(128)}, u32[]{:S(2)}) copy-start(f32[128]{0:T(128)} %param.27) | copy-start | bytes 1540
  179.2 35.9 %all-to-all-start.2 = ((bf16[128,3,2048]{2,1,0:T(4,128)(2,1)}), bf16[128,3,2048]{2,1,0:T(4,128)(2,1)}, u32[]{:S(2)}, u32[]{:S(2)}) async-start(bf16[128,3,2048]{2,1,0:T(4,128)(2,1)} %reshape.233), calls=%async_computation.2 | async-start | bytes 4194304 | tf_op jit(solution)/shard_map/all_to_all | solution.py:164
  226.8 1.5 copy-start.2
where the time goes:
time: 231 us; the launch traced here: 230 us
  blocking collectives  96 us (42%)
  local copies, waits for them, and re-layouts  41.8 us (18%)
  waiting for transfers between devices  30.9 us (13%)
  starting transfers between devices  25.3 us (11%)
  other arithmetic  18.6 us (8%)
  matrix products  16.7 us (7%)
    all_gather x6, blocking collectives, entering_2(): pieces = jax.tree.map(lambda part: lax.all_gather(part, axis), so_far)  59.1 us
    all_to_all x1, blocking collectives, local(): lax.all_to_all(outgoing, SP_TP, split_axis=0, concat_axis=0, tiled=True)  36.9 us
    all_to_all x1, waiting for transfers between devices, local(): lax.all_to_all(served.reshape(shape_in), SP_TP, split_axis=0, concat_axis...  30.2 us
    all_to_all x1, starting transfers between devices, local(): lax.all_to_all(mixer_out, 'tp', split_axis=0, concat_axis=1, tiled=True)  19.7 us
    reshape x2, local copies, waits for them, and re-layouts, local(): returned.reshape(experts_total * capacity, model_width)[slot_index]  6.78 us
    all_to_all x1, starting transfers between devices, local(): lax.all_to_all(served.reshape(shape_in), SP_TP, split_axis=0, concat_axis...  5.6 us
    dot_general x1, matrix products, expert_apply(): jnp.dot(inner_rows, down_matrix, preferred_element_type=jnp.float32)  5.2 us
    reshape x1, local copies, waits for them, and re-layouts, local(): outgoing = padded[owners].reshape(experts_total, capacity, model_width)  5.15 us
  transfers between devices with their start and end apart: 2, of which 2 were waited for; matrix products, arithmetic and copies ran while one was open for 0% of the time, Pallas kernels for 0%

commit v1 on v0

v1 whole, which is shorter than its diff:
```python
import jax
import jax.numpy as jnp
from jax import lax
from jax.experimental import pallas as pl
from jax.experimental.pallas import tpu as pltpu
from jax.sharding import Mesh
from jax.sharding import PartitionSpec as P

AXES = ("sp_0", "sp_1", "sp_2", "tp")
SP = AXES[:3]
MESH = pl.DeviceIdType.MESH
F32, BF16, I32 = jnp.float32, jnp.bfloat16, jnp.int32

BLOCK = 64
SEG = 256
ROWS = 128
HEADS = 4
PAIRS = HEADS // 2
WIDTH = 2048
CHUNKS = WIDTH // 128
HIDDEN = 512
DEVICES = 128
CAP = 3
SLOTS = DEVICES * CAP


def dot(a, b, dims=((1,), (0,))):
    return lax.dot_general(a, b, (dims, ((), ())), preferred_element_type=F32)


def split3(x):
    high = x.astype(BF16)
    rest = x - high.astype(F32)
    mid = rest.astype(BF16)
    return high, mid, (rest - mid.astype(F32)).astype(BF16)


def iota(shape, dim):
    return lax.broadcasted_iota(I32, shape, dim)


def silu(x):
    return x / (1.0 + jnp.exp(-x))


def kernel(
    residual, queries, keys, values, out_gate, gate_logits, head_gain, out_weight, norm_gain,
    routes, group_score, expert_score, gate_weight, up_weight, down_weight,
    out,
    q_v, k_v, v_v, og_v, gl_v, res_v, ow_v, gw_v, uw_v, dw_v,
    f_v, qd_v, att_v, gain_v, mix_v, pair_v, states, decays, perm_v, pick_v, comb_v,
    merged_v, norm_v, nat_v, send_v, recv_v, inner_v, back_v, ret_v,
    in_sem, w_sem, s_send, s_recv, d_send, d_recv, p_send, p_recv, x_send, x_recv, y_send, y_recv,
):
    place = [lax.axis_index(axis) for axis in AXES]
    core = place[3]
    me = ((place[0] * 4 + place[1]) * 4 + place[2]) * 2 + core

    def shifted(axis, step):
        there = list(place)
        size = 2 if axis == 3 else 4
        there[axis] = (place[axis] + step) % size
        return tuple(there)

    def fetch(pairs, sems, first):
        copies = [
            pltpu.make_async_copy(src, dst, sems.at[first + i]) for i, (src, dst) in enumerate(pairs)
        ]
        for copy in copies:
            copy.start()
        return copies

    get_gl, get_k, get_v, get_q, get_og, get_res = fetch(
        (
            (gate_logits, gl_v), (keys, k_v), (values, v_v), (queries, q_v), (out_gate, og_v),
            (residual, res_v),
        ),
        in_sem,
        0,
    )
    get_ow, get_gw, get_uw, get_dw = fetch(
        (
            (out_weight, ow_v), (gate_weight.at[0], gw_v), (up_weight.at[0], uw_v),
            (down_weight.at[0], dw_v),
        ),
        w_sem,
        0,
    )

    barrier = pltpu.get_barrier_semaphore()
    friends = [(axis, step) for axis in range(3) for step in (1, 2, 3)] + [(3, 1)]
    for axis, step in friends:
        pl.semaphore_signal(
            barrier, inc=1, device_id=shifted(axis, step), device_id_type=MESH
        )

    get_gl.wait()
    x = -gl_v[...].astype(F32)
    decay = -(jnp.maximum(x, 0.0) + jnp.log1p(jnp.exp(-jnp.abs(x)))) * (1.0 / 16.0)
    lower = jnp.where(iota((SEG, SEG), 0) >= iota((SEG, SEG), 1), 1.0, 0.0).astype(BF16)
    high, mid, low = split3(decay)
    f_v[...] = (dot(lower, low) + dot(lower, mid)) + dot(lower, high)

    def end_row(n):
        return f_v[pl.ds(n * BLOCK - 1, 1), :]

    lane_low = iota((1, 128), 1) < 64

    def state_after(n):
        rows = n * BLOCK
        aged = k_v[0:rows, :].astype(F32) * jnp.exp(end_row(n) - f_v[0:rows, :])
        aged = aged.astype(BF16)
        pairs = []
        for p in range(PAIRS):
            side = [
                dot(
                    v_v[0:rows, (2 * p + i) * 128 : (2 * p + i + 1) * 128],
                    aged[:, p * 128 : (p + 1) * 128],
                    ((0,), (0,)),
                )
                for i in range(2)
            ]
            pairs.append(jnp.where(lane_low, side[0], side[1]))
        return pairs

    get_k.wait()
    get_v.wait()
    local_end = state_after(SEG // BLOCK)
    spot = place[2]
    for p in range(PAIRS):
        states[2, spot, :, p * 128 : (p + 1) * 128] = local_end[p].astype(BF16)
    decays[2, spot] = jnp.broadcast_to(end_row(SEG // BLOCK), (8, 256))
    pl.semaphore_wait(barrier, len(friends))

    def share(level):
        here = place[level]
        for step in (2, 1, 3):
            for buf, ss, rs in ((states, s_send, s_recv), (decays, d_send, d_recv)):
                pltpu.make_async_remote_copy(
                    src_ref=buf.at[level, here],
                    dst_ref=buf.at[level, here],
                    send_sem=ss.at[level],
                    recv_sem=rs.at[level],
                    device_id=shifted(level, step),
                    device_id_type=MESH,
                ).start()

    def await_share(level):
        for buf, ss, rs in ((states, s_send, s_recv), (decays, d_send, d_recv)):
            three = buf.at[level, pl.ds(0, 3)]
            pltpu.make_async_copy(three, three, rs.at[level]).wait()
            pltpu.make_async_copy(three, three, ss.at[level]).wait()

    def run_line(level):
        here = place[level]
        state = jnp.zeros((128, 256), F32)
        total = jnp.zeros((1, 256), F32)
        enter, before = state, total
        for j in range(4):
            enter = jnp.where(here == j, state, enter)
            before = jnp.where(here == j, total, before)
            step = decays[level, j, 0:1, :]
            state = state * jnp.exp(step) + states[level, j].astype(F32)
            total = total + step
        return enter, before, state, total

    share(2)

    get_q.wait()
    scale = 64.0 ** (-0.5)
    block_row = iota((SEG, 1), 0) // BLOCK
    f = f_v[...]
    start = jnp.zeros((SEG, 256), F32)
    for n in range(1, SEG // BLOCK):
        start = jnp.where(block_row == n, end_row(n), start)
    running = f - start
    q = q_v[...].astype(F32) * scale
    qd_v[...] = (q * jnp.exp(f)).astype(BF16)
    q_scaled = (q * jnp.exp(running)).astype(BF16)
    k_inverse = (k_v[...].astype(F32) * jnp.exp(-running)).astype(BF16)
    row, col = iota((SEG, SEG), 0), iota((SEG, SEG), 1)
    causal = (row >= col) & (row // BLOCK == col // BLOCK)
    none = jnp.zeros((), BF16)
    local_states = [None] + [
        [s.astype(BF16) for s in state_after(n)] for n in range(1, SEG // BLOCK)
    ]
    for h in range(HEADS):
        p = h // 2
        mine = lane_low if h % 2 == 0 else jnp.logical_not(lane_low)
        lanes = slice(p * 128, (p + 1) * 128)
        q_h = jnp.where(mine, q_scaled[:, lanes], none)
        k_h = jnp.where(mine, k_inverse[:, lanes], none)
        scores = jnp.where(causal, dot(q_h, k_h, ((1,), (1,))), 0.0).astype(BF16)
        here = slice(h * 128, (h + 1) * 128)
        att_v[:, here] = dot(scores, v_v[:, here])
        for n in range(1, SEG // BLOCK):
            rows = slice(n * BLOCK, (n + 1) * BLOCK)
            att_v[rows, here] += dot(q_h[rows], local_states[n][p], ((1,), (1,)))
    get_og.wait()
    for h in range(HEADS):
        here = slice(h * 128, (h + 1) * 128)
        gain_v[:, here] = silu(og_v[:, here].astype(F32)) * head_gain[...]

    diagonal = iota((128, 128), 0) == iota((128, 128), 1)

    def as_row(column):
        return jnp.sum(jnp.where(diagonal, column, 0.0), axis=0, keepdims=True)

    def as_column(line):
        return jnp.sum(jnp.where(diagonal, line, 0.0), axis=1, keepdims=True)

    expert_id = iota((128, 128), 0).astype(F32)
    earlier = jnp.where(iota((128, 128), 0) < iota((128, 128), 1), 1.0, 0.0).astype(BF16)
    taken = jnp.zeros((128, 1), F32)
    slot_rows = []
    for c in range(2):
        line = as_row(routes[:, c : c + 1].astype(F32))
        hit = jnp.where(expert_id == line, 1.0, 0.0)
        count = dot(hit.astype(BF16), earlier) + taken
        rank = jnp.sum(hit * count, axis=0, keepdims=True)
        slot_rows.append(line * CAP + rank)
        taken = taken + jnp.sum(hit, axis=1, keepdims=True)
    slot_id = iota((SLOTS, 128), 0).astype(F32)
    pick_v[...] = (
        jnp.where(slot_id == slot_rows[0], 1.0, 0.0) + jnp.where(slot_id == slot_rows[1], 1.0, 0.0)
    ).astype(BF16)
    score = expert_score[...]
    score_sum = score[:, 0:1] + score[:, 1:2]
    group = as_column(group_score[...])
    slot_lane = iota((ROWS, SLOTS), 1).astype(F32)
    comb = jnp.zeros((ROWS, SLOTS), F32)
    for c in range(2):
        weight = group * score[:, c : c + 1] / score_sum
        comb = comb + jnp.where(slot_lane == as_column(slot_rows[c]), weight, 0.0)
    for i, part in enumerate(split3(comb)[:2]):
        comb_v[i] = part
    row, col = iota((256, 256), 0), iota((256, 256), 1)
    perm_v[...] = jnp.where(row == (col % 16) * 16 + col // 16, 1.0, 0.0).astype(BF16)

    entering = None
    scales = []
    enters = []
    for level in (2, 1, 0):
        await_share(level)
        enter, before, state, total = run_line(level)
        if level:
            upper = level - 1
            states[upper, place[upper]] = state.astype(BF16)
            decays[upper, place[upper]] = jnp.broadcast_to(total, (8, 256))
            share(upper)
        enters.append(enter)
        scales.append(jnp.exp(before))
    entering = enters[0] + scales[0] * (enters[1] + scales[1] * enters[2])
    entering = entering.astype(BF16)

    for h in range(HEADS):
        p = h // 2
        mine = lane_low if h % 2 == 0 else jnp.logical_not(lane_low)
        lanes = slice(p * 128, (p + 1) * 128)
        here = slice(h * 128, (h + 1) * 128)
        q_h = jnp.where(mine, qd_v[:, lanes], none)
        attended = att_v[:, here] + dot(q_h, entering[:, lanes], ((1,), (1,)))
        mean = jnp.mean(attended * attended, axis=-1, keepdims=True)
        mix_v[:, here] = (attended * lax.rsqrt(mean + 1e-06) * gain_v[:, here]).astype(BF16)
    other_rows = pl.ds(pl.multiple_of((1 - core) * ROWS, ROWS), ROWS)
    own_rows = pl.ds(pl.multiple_of(core * ROWS, ROWS), ROWS)
    swap = pltpu.make_async_remote_copy(
        src_ref=mix_v.at[other_rows],
        dst_ref=pair_v,
        send_sem=p_send,
        recv_sem=p_recv,
        device_id=shifted(3, 1),
        device_id_type=MESH,
    )
    swap.start()
    get_res.wait()
    get_ow.wait()
    half = HEADS * 128
    own_w = pl.ds(pl.multiple_of(core * half, half), half)
    other_w = pl.ds(pl.multiple_of((1 - core) * half, half), half)
    summed = res_v[...].astype(F32) + dot(mix_v[own_rows, :], ow_v[own_w, :])
    swap.wait()
    summed = summed + dot(pair_v[...], ow_v[other_w, :])
    merged = summed.astype(BF16)
    merged_v[...] = merged
    wide = merged.astype(F32)
    mean = jnp.mean(wide * wide, axis=-1, keepdims=True)
    norm_v[...] = (wide * lax.rsqrt(mean + 1e-06) * norm_gain[...]).astype(BF16)

    nat_v[...] = dot(pick_v[...], norm_v[...]).astype(BF16)

    def to_tiles(src, dst):
        @pl.loop(0, SLOTS // 16)
        def _(g):
            rows = pl.ds(pl.multiple_of(g * 16, 16), 16)
            stack = jnp.concatenate(
                [src[rows, j * 128 : (j + 1) * 128] for j in range(CHUNKS)], axis=0
            )
            moved = dot(perm_v[...], stack).astype(BF16)
            dst[rows] = moved.reshape(16, CHUNKS, 128)

    def from_tiles(src, dst):
        @pl.loop(0, SLOTS // 16)
        def _(g):
            rows = pl.ds(pl.multiple_of(g * 16, 16), 16)
            moved = dot(perm_v[...], src[rows].reshape(16 * CHUNKS, 128)).astype(BF16)
            for j in range(CHUNKS):
                dst[rows, j * 128 : (j + 1) * 128] = moved[j * 16 : (j + 1) * 16]

    def exchange(src, dst, ss, rs):
        @pl.loop(1, DEVICES)
        def _(i):
            offset = (i * 53) % DEVICES
            steps = (offset // 32, (offset // 8) % 4, (offset // 2) % 4, offset % 2)
            there = tuple(
                (place[a] + steps[a]) % (2 if a == 3 else 4) for a in range(4)
            )
            peer = ((there[0] * 4 + there[1]) * 4 + there[2]) * 2 + there[3]
            pltpu.make_async_remote_copy(
                src_ref=src.at[pl.ds(peer * CAP, CAP)],
                dst_ref=dst.at[pl.ds(me * CAP, CAP)],
                send_sem=ss,
                recv_sem=rs,
                device_id=there,
                device_id_type=MESH,
            ).start()

        mine = pl.ds(me * CAP, CAP)
        dst[mine] = src[mine]

    def await_exchange(src, dst, ss, rs):
        most = pl.ds(0, (DEVICES - 1) * CAP)
        pltpu.make_async_copy(src.at[most], dst.at[most], rs).wait()
        pltpu.make_async_copy(src.at[most], dst.at[most], ss).wait()

    to_tiles(nat_v, send_v)
    exchange(send_v, recv_v, x_send, x_recv)
    get_gw.wait()
    get_uw.wait()
    get_dw.wait()
    await_exchange(send_v, recv_v, x_send, x_recv)
    from_tiles(recv_v, nat_v)

    @pl.loop(0, HIDDEN // 256)
    def _(n):
        cols = pl.ds(pl.multiple_of(n * 256, 256), 256)
        gated = dot(nat_v[...], gw_v[:, cols])
        lifted = dot(nat_v[...], uw_v[:, cols])
        inner_v[:, cols] = (silu(gated) * lifted).astype(BF16)

    @pl.loop(0, WIDTH // 256)
    def _(n):
        cols = pl.ds(pl.multiple_of(n * 256, 256), 256)
        nat_v[:, cols] = dot(inner_v[...], dw_v[:, cols]).astype(BF16)

    to_tiles(nat_v, back_v)
    exchange(back_v, ret_v, y_send, y_recv)
    await_exchange(back_v, ret_v, y_send, y_recv)
    from_tiles(ret_v, nat_v)

    @pl.loop(0, WIDTH // 256)
    def _(n):
        cols = pl.ds(pl.multiple_of(n * 256, 256), 256)
        combined = dot(comb_v[1], nat_v[:, cols]) + dot(comb_v[0], nat_v[:, cols])
        out[:, cols] = (merged_v[:, cols].astype(F32) + combined).astype(BF16)


def local(
    residual, queries, key_rows, value_rows, out_gate, gate_logits, head_gain, out_weight,
    norm_gain, routes, group_score, expert_score, gate_weight, up_weight, down_weight,
):
    anywhere = pl.BlockSpec(memory_space=pl.ANY)
    vmem = pl.BlockSpec(memory_space=pltpu.VMEM)
    half = HEADS * 128
    tiles = pltpu.VMEM((SLOTS, CHUNKS, 128), BF16)
    dma = pltpu.SemaphoreType.DMA
    return pl.pallas_call(
        kernel,
        out_shape=jax.ShapeDtypeStruct((ROWS, WIDTH), BF16),
        in_specs=[anywhere] * 6 + [vmem, anywhere, vmem, vmem, vmem, vmem] + [anywhere] * 3,
        out_specs=vmem,
        scratch_shapes=[
            pltpu.VMEM((SEG, 256), BF16),
            pltpu.VMEM((SEG, 256), BF16),
            pltpu.VMEM((SEG, half), BF16),
            pltpu.VMEM((SEG, half), BF16),
            pltpu.VMEM((SEG, 256), BF16),
            pltpu.VMEM((ROWS, WIDTH), BF16),
            pltpu.VMEM((2 * half, WIDTH), BF16),
            pltpu.VMEM((WIDTH, HIDDEN), BF16),
            pltpu.VMEM((WIDTH, HIDDEN), BF16),
            pltpu.VMEM((HIDDEN, WIDTH), BF16),
            pltpu.VMEM((SEG, 256), F32),
            pltpu.VMEM((SEG, 256), BF16),
            pltpu.VMEM((SEG, half), F32),
            pltpu.VMEM((SEG, half), F32),
            pltpu.VMEM((SEG, half), BF16),
            pltpu.VMEM((ROWS, half), BF16),
            pltpu.VMEM((3, 4, 128, 256), BF16),
            pltpu.VMEM((3, 4, 8, 256), F32),
            pltpu.VMEM((256, 256), BF16),
            pltpu.VMEM((SLOTS, ROWS), BF16),
            pltpu.VMEM((2, ROWS, SLOTS), BF16),
            pltpu.VMEM((ROWS, WIDTH), BF16),
            pltpu.VMEM((ROWS, WIDTH), BF16),
            pltpu.VMEM((SLOTS, WIDTH), BF16),
            tiles,
            tiles,
            pltpu.VMEM((SLOTS, HIDDEN), BF16),
            tiles,
            tiles,
            dma((6,)), dma((4,)),
            dma((3,)), dma((3,)), dma((3,)), dma((3,)),
            dma, dma, dma, dma, dma, dma,
        ],
        compiler_params=pltpu.CompilerParams(
            collective_id=0, has_side_effects=True, vmem_limit_bytes=56 * 2**20
        ),
    )(
        residual, queries, key_rows, value_rows, out_gate, gate_logits,
        head_gain.reshape(1, 128), out_weight, norm_gain.reshape(1, WIDTH),
        routes, group_score.reshape(1, ROWS), expert_score, gate_weight, up_weight, down_weight,
    )


def solution(mesh):
    torus = Mesh(mesh.devices.reshape(4, 4, 4, mesh.shape["tp"]), AXES)
    both = P(AXES)
    in_specs = (
        P(AXES, None),
        P(SP, "tp"), P(SP, "tp"), P(SP, "tp"), P(SP, "tp"), P(SP, "tp"),
        P(), P(), P(),
        P(AXES, None), both, P(AXES, None),
        P(AXES, None, None), P(AXES, None, None), P(AXES, None, None),
    )
    return jax.shard_map(
        local, mesh=torus, in_specs=in_specs, out_specs=P(AXES, None), check_vma=False
    )
```

time: 231 us -> 97.8 us (0.42)
  blocking collectives: 96 us -> 0 us
  Pallas kernels: 0 us -> 92.8 us
  local copies, waits for them, and re-layouts: 41.8 us -> 4.7 us
  waiting for transfers between devices: 30.9 us -> 0 us
  starting transfers between devices: 25.3 us -> 0 us
  other arithmetic: 18.6 us -> 0 us
  matrix products: 16.7 us -> 0 us
    pallas_call x0 -> x1, Pallas kernels: none -> 92.8 us  [local(): pl.pallas_call(kernel, out_shape=jax.ShapeDtypeStruct((ROWS, WIDTH), BF16...]
    all_gather x6 -> x0, blocking collectives: 59.1 us -> none  [entering_2(): pieces = jax.tree.map(lambda part: lax.all_gather(part, axis), so_far)]
    all_to_all x1 -> x0, blocking collectives: 36.9 us -> none  [local(): lax.all_to_all(outgoing, SP_TP, split_axis=0, concat_axis=0, tiled=True)]
    all_to_all x2 -> x0, waiting for transfers between devices: 30.9 us -> none  [the longest x1 30.2 us: local(): lax.all_to_all(served.reshape(shape_in), SP_TP, split_axis=0, concat_axis...]
    all_to_all x2 -> x0, starting transfers between devices: 25.3 us -> none  [the longest x1 19.7 us: local(): lax.all_to_all(mixer_out, 'tp', split_axis=0, concat_axis=1, tiled=True)]
    reshape x8 -> x0, local copies, waits for them, and re-layouts: 23.4 us -> none  [the longest x2 6.78 us: local(): returned.reshape(experts_total * capacity, model_width)[slot_index]]
    dot_general x7 -> x0, matrix products: 16.7 us -> none  [the longest x1 5.2 us: expert_apply(): jnp.dot(inner_rows, down_matrix, preferred_element_type=jnp.float32)]
    gather x2 -> x0, local copies, waits for them, and re-layouts: 8.06 us -> none  [the longest x1 4.96 us: local(): returned.reshape(experts_total * capacity, model_width)[slot_index]]
  transfers between devices with their start and end apart: 2 -> 0, of which waited for: 2 -> 0; matrix products, arithmetic and copies ran while one was open for 0% -> 0% of each run, Pallas kernels for 0% -> 0%
where the time goes in v1:
time: 97.8 us; the launch traced here: 97.6 us
  Pallas kernels  92.8 us (95%)
  local copies, waits for them, and re-layouts  4.7 us (5%)
    pallas_call x1, Pallas kernels, local(): pl.pallas_call(kernel, out_shape=jax.ShapeDtypeStruct((ROWS, WIDTH), BF16...  92.8 us
    unnamed x3, local copies, waits for them, and re-layouts  4.7 us

profile of v1, /device:TPU:1, one launch (start us, length us, event | category | flops | bytes accessed | tf_op | source)
XLA Modules:
  0.0 97.6 jit_solution(10257925155946953031)
XLA Ops:
  0.0 1.4 %copy.16.routes = s32[128,2]{1,0:T(8,128)} copy(s32[128,2]{0,1:T(2,128)} %param.24) | data formatting | bytes 2048 | tf_op args[9]
  1.4 1.4 %copy.17.expert_score = f32[128,2]{1,0:T(8,128)} copy(f32[128,2]{0,1:T(2,128)} %param.26) | data formatting | bytes 2048 | tf_op args[11]
  2.8 92.8 %shard_map.145 = bf16[128,2048]{1,0:T(8,128)(2,1)} custom-call(bf16[128,2048]{1,0:T(8,128)(2,1)} %residual.1, bf16[256,256]{1,0:T(8,128)(2,1)} %queries.1, bf16[256,256]{1,0:T(8,128)(2,1)} %keys.1, bf16[256,512]{1,0:T(8,128)(2,1)} %values.1, bf16[256,512]{1,0:T(8,128)(2,1)} %out_gate.1, bf16[256,256]{1,0:T(8,128)(2,1)} %gate_logits.1, f32[1,128]{1,0:T(1,128)} %bitcast.4, ...), custom_call_target="tpu_custom_call" | custom-call | tf_op jit(solution)/shard_map/pallas_call | solution.py:377
  95.7 1.9 %copy.19 = bf16[128,2048]{1,0:T(8,128)(2,1)} copy(bf16[128,2048]{1,0:T(8,128)(2,1)} %shard_map.145) | data formatting | bytes 1048576

commit v2 on v1

--- a/solution.py
+++ b/solution.py
@@ -22,6 +22,11 @@
 DEVICES = 128
 CAP = 3
 SLOTS = DEVICES * CAP
+PARTS = 4
+STEPS = DEVICES // PARTS
+PART = STEPS * CAP
+STRIDE, UNSTRIDE = 53, 29
+PITCH = CHUNKS + 1
 
 
 def dot(a, b, dims=((1,), (0,))):
@@ -48,8 +53,8 @@
     routes, group_score, expert_score, gate_weight, up_weight, down_weight,
     out,
     q_v, k_v, v_v, og_v, gl_v, res_v, ow_v, gw_v, uw_v, dw_v,
-    f_v, qd_v, att_v, gain_v, mix_v, pair_v, states, decays, perm_v, pick_v, comb_v,
-    merged_v, norm_v, nat_v, send_v, recv_v, inner_v, back_v, ret_v,
+    f_v, qd_v, att_v, gain_v, mix_v, pair_v, states, decays, pick_v, comb_v,
+    norm_v, acc_v, nat_v, tile_v, send_v, recv_v, inner_v, back_v, ret_v,
     in_sem, w_sem, s_send, s_recv, d_send, d_recv, p_send, p_recv, x_send, x_recv, y_send, y_recv,
 ):
     place = [lax.axis_index(axis) for axis in AXES]
@@ -203,39 +208,41 @@
 
     diagonal = iota((128, 128), 0) == iota((128, 128), 1)
 
-    def as_row(column):
-        return jnp.sum(jnp.where(diagonal, column, 0.0), axis=0, keepdims=True)
-
     def as_column(line):
         return jnp.sum(jnp.where(diagonal, line, 0.0), axis=1, keepdims=True)
 
-    expert_id = iota((128, 128), 0).astype(F32)
+    expert_id = iota((128, 128), 0)
     earlier = jnp.where(iota((128, 128), 0) < iota((128, 128), 1), 1.0, 0.0).astype(BF16)
     taken = jnp.zeros((128, 1), F32)
     slot_rows = []
     for c in range(2):
-        line = as_row(routes[:, c : c + 1].astype(F32))
+        line = routes[c : c + 1, :]
         hit = jnp.where(expert_id == line, 1.0, 0.0)
         count = dot(hit.astype(BF16), earlier) + taken
         rank = jnp.sum(hit * count, axis=0, keepdims=True)
-        slot_rows.append(line * CAP + rank)
+        offset = jnp.zeros_like(line)
+        for a, unit in enumerate((32, 8, 2, 1)):
+            size = 2 if a == 3 else 4
+            offset = offset + unit * ((line // unit % size - place[a] + size) % size)
+        step = offset * UNSTRIDE % DEVICES
+        slot_rows.append((step * CAP).astype(F32) + rank)
         taken = taken + jnp.sum(hit, axis=1, keepdims=True)
     slot_id = iota((SLOTS, 128), 0).astype(F32)
     pick_v[...] = (
         jnp.where(slot_id == slot_rows[0], 1.0, 0.0) + jnp.where(slot_id == slot_rows[1], 1.0, 0.0)
     ).astype(BF16)
-    score = expert_score[...]
-    score_sum = score[:, 0:1] + score[:, 1:2]
+    score = [as_column(expert_score[c : c + 1, :]) for c in range(2)]
     group = as_column(group_score[...])
-    slot_lane = iota((ROWS, SLOTS), 1).astype(F32)
-    comb = jnp.zeros((ROWS, SLOTS), F32)
-    for c in range(2):
-        weight = group * score[:, c : c + 1] / score_sum
-        comb = comb + jnp.where(slot_lane == as_column(slot_rows[c]), weight, 0.0)
-    for i, part in enumerate(split3(comb)[:2]):
-        comb_v[i] = part
-    row, col = iota((256, 256), 0), iota((256, 256), 1)
-    perm_v[...] = jnp.where(row == (col % 16) * 16 + col // 16, 1.0, 0.0).astype(BF16)
+    slot_columns = [as_column(line) for line in slot_rows]
+    for part in range(PARTS):
+        slot_lane = (iota((ROWS, PART), 1) + part * PART).astype(F32)
+        comb = jnp.zeros((ROWS, PART), F32)
+        for c in range(2):
+            weight = group * score[c] / (score[0] + score[1])
+            comb = comb + jnp.where(slot_lane == slot_columns[c], weight, 0.0)
+        high, mid, _ = split3(comb)
+        comb_v[part, 0:ROWS] = mid
+        comb_v[part, ROWS : 2 * ROWS] = high
 
     entering = None
     scales = []
@@ -281,88 +288,93 @@
     summed = res_v[...].astype(F32) + dot(mix_v[own_rows, :], ow_v[own_w, :])
     swap.wait()
     summed = summed + dot(pair_v[...], ow_v[other_w, :])
-    merged = summed.astype(BF16)
-    merged_v[...] = merged
-    wide = merged.astype(F32)
+    wide = summed.astype(BF16).astype(F32)
+    acc_v[...] = wide
     mean = jnp.mean(wide * wide, axis=-1, keepdims=True)
     norm_v[...] = (wide * lax.rsqrt(mean + 1e-06) * norm_gain[...]).astype(BF16)
 
-    nat_v[...] = dot(pick_v[...], norm_v[...]).astype(BF16)
-
-    def to_tiles(src, dst):
-        @pl.loop(0, SLOTS // 16)
+    def put_columns(j, block):
+        for i in range(2):
+            tile_v[pl.ds(2 * j + i, PART, stride=PITCH), :] = block[:, i * 128 : (i + 1) * 128]
+
+    def gather_tiles(dst, part):
+        @pl.loop(0, PART // 16)
         def _(g):
-            rows = pl.ds(pl.multiple_of(g * 16, 16), 16)
-            stack = jnp.concatenate(
-                [src[rows, j * 128 : (j + 1) * 128] for j in range(CHUNKS)], axis=0
+            for i in range(16):
+                slot = g * 16 + i
+                dst[part * PART + slot] = tile_v[pl.ds(slot * PITCH, CHUNKS), :].astype(BF16)
+
+    def to_rows(src, part):
+        @pl.loop(0, PART // 32)
+        def _(g):
+            for i in range(2):
+                rows = pl.ds(pl.multiple_of(g * 32 + i * 16, 16), 16)
+                nat_v[rows, :] = src[pl.ds(part * PART + g * 32 + i * 16, 16)].reshape(16, WIDTH)
+
+    def send_part(part, src, dst, ss, rs, sign):
+        @pl.loop(max(1, part * STEPS), (part + 1) * STEPS)
+        def _(i):
+            offset = lax.rem(i * STRIDE, DEVICES)
+            steps = (
+                lax.div(offset, 32), lax.rem(lax.div(offset, 8), 4), lax.rem(lax.div(offset, 2), 4),
+                lax.rem(offset, 2),
             )
-            moved = dot(perm_v[...], stack).astype(BF16)
-            dst[rows] = moved.reshape(16, CHUNKS, 128)
-
-    def from_tiles(src, dst):
-        @pl.loop(0, SLOTS // 16)
-        def _(g):
-            rows = pl.ds(pl.multiple_of(g * 16, 16), 16)
-            moved = dot(perm_v[...], src[rows].reshape(16 * CHUNKS, 128)).astype(BF16)
-            for j in range(CHUNKS):
-                dst[rows, j * 128 : (j + 1) * 128] = moved[j * 16 : (j + 1) * 16]
-
-    def exchange(src, dst, ss, rs):
-        @pl.loop(1, DEVICES)
-        def _(i):
-            offset = (i * 53) % DEVICES
-            steps = (offset // 32, (offset // 8) % 4, (offset // 2) % 4, offset % 2)
             there = tuple(
-                (place[a] + steps[a]) % (2 if a == 3 else 4) for a in range(4)
+                lax.rem(place[a] + sign * steps[a] + 4, 2 if a == 3 else 4) for a in range(4)
             )
-            peer = ((there[0] * 4 + there[1]) * 4 + there[2]) * 2 + there[3]
+            rows = pl.ds(i * CAP, CAP)
             pltpu.make_async_remote_copy(
-                src_ref=src.at[pl.ds(peer * CAP, CAP)],
-                dst_ref=dst.at[pl.ds(me * CAP, CAP)],
+                src_ref=src.at[rows],
+                dst_ref=dst.at[rows],
                 send_sem=ss,
-                recv_sem=rs,
+                recv_sem=rs.at[part],
                 device_id=there,
                 device_id_type=MESH,
             ).start()
 
-        mine = pl.ds(me * CAP, CAP)
-        dst[mine] = src[mine]
-
-    def await_exchange(src, dst, ss, rs):
-        most = pl.ds(0, (DEVICES - 1) * CAP)
-        pltpu.make_async_copy(src.at[most], dst.at[most], rs).wait()
-        pltpu.make_async_copy(src.at[most], dst.at[most], ss).wait()
-
-    to_tiles(nat_v, send_v)
-    exchange(send_v, recv_v, x_send, x_recv)
+        if part == 0:
+            dst[0:CAP] = src[0:CAP]
+
+    def await_part(part, dst, rs):
+        count = PART - (CAP if part == 0 else 0)
+        rows = dst.at[pl.ds(part * PART, count)]
+        pltpu.make_async_copy(rows, rows, rs.at[part]).wait()
+
+    for part in range(PARTS):
+        chosen = pick_v[part * PART : (part + 1) * PART, :]
+        for j in range(WIDTH // 256):
+            put_columns(j, dot(chosen, norm_v[:, j * 256 : (j + 1) * 256]))
+        gather_tiles(send_v, part)
+        send_part(part, send_v, recv_v, x_send, x_recv, 1)
     get_gw.wait()
     get_uw.wait()
     get_dw.wait()
-    await_exchange(send_v, recv_v, x_send, x_recv)
-    from_tiles(recv_v, nat_v)
-
-    @pl.loop(0, HIDDEN // 256)
-    def _(n):
-        cols = pl.ds(pl.multiple_of(n * 256, 256), 256)
-        gated = dot(nat_v[...], gw_v[:, cols])
-        lifted = dot(nat_v[...], uw_v[:, cols])
-        inner_v[:, cols] = (silu(gated) * lifted).astype(BF16)
-
-    @pl.loop(0, WIDTH // 256)
-    def _(n):
-        cols = pl.ds(pl.multiple_of(n * 256, 256), 256)
-        nat_v[:, cols] = dot(inner_v[...], dw_v[:, cols]).astype(BF16)
-
-    to_tiles(nat_v, back_v)
-    exchange(back_v, ret_v, y_send, y_recv)
-    await_exchange(back_v, ret_v, y_send, y_recv)
-    from_tiles(ret_v, nat_v)
-
-    @pl.loop(0, WIDTH // 256)
-    def _(n):
-        cols = pl.ds(pl.multiple_of(n * 256, 256), 256)
-        combined = dot(comb_v[1], nat_v[:, cols]) + dot(comb_v[0], nat_v[:, cols])
-        out[:, cols] = (merged_v[:, cols].astype(F32) + combined).astype(BF16)
+    for part in range(PARTS):
+        await_part(part, recv_v, x_recv)
+        to_rows(recv_v, part)
+        for n in range(HIDDEN // 256):
+            cols = slice(n * 256, (n + 1) * 256)
+            gated = dot(nat_v[...], gw_v[:, cols])
+            lifted = dot(nat_v[...], uw_v[:, cols])
+            inner_v[:, cols] = (silu(gated) * lifted).astype(BF16)
+        for j in range(WIDTH // 256):
+            put_columns(j, dot(inner_v[...], dw_v[:, j * 256 : (j + 1) * 256]))
+        gather_tiles(back_v, part)
+        send_part(part, back_v, ret_v, y_send, y_recv, -1)
+    for part in range(PARTS):
+        await_part(part, ret_v, y_recv)
+        to_rows(ret_v, part)
+        for j in range(WIDTH // 256):
+            cols = slice(j * 256, (j + 1) * 256)
+            both = dot(comb_v[part], nat_v[:, cols])
+            total = acc_v[:, cols] + (both[0:ROWS] + both[ROWS : 2 * ROWS])
+            if part < PARTS - 1:
+                acc_v[:, cols] = total
+            else:
+                out[:, cols] = total.astype(BF16)
+    for src, ss in ((send_v, x_send), (back_v, y_send)):
+        rows = src.at[pl.ds(0, SLOTS - CAP)]
+        pltpu.make_async_copy(rows, rows, ss).wait()
 
 
 def local(
@@ -398,20 +410,20 @@
             pltpu.VMEM((ROWS, half), BF16),
             pltpu.VMEM((3, 4, 128, 256), BF16),
             pltpu.VMEM((3, 4, 8, 256), F32),
-            pltpu.VMEM((256, 256), BF16),
             pltpu.VMEM((SLOTS, ROWS), BF16),
-            pltpu.VMEM((2, ROWS, SLOTS), BF16),
+            pltpu.VMEM((PARTS, 2 * ROWS, PART), BF16),
             pltpu.VMEM((ROWS, WIDTH), BF16),
-            pltpu.VMEM((ROWS, WIDTH), BF16),
-            pltpu.VMEM((SLOTS, WIDTH), BF16),
+            pltpu.VMEM((ROWS, WIDTH), F32),
+            pltpu.VMEM((PART, WIDTH), BF16),
+            pltpu.VMEM((PART * PITCH, 128), F32),
             tiles,
             tiles,
-            pltpu.VMEM((SLOTS, HIDDEN), BF16),
+            pltpu.VMEM((PART, HIDDEN), BF16),
             tiles,
             tiles,
             dma((6,)), dma((4,)),
             dma((3,)), dma((3,)), dma((3,)), dma((3,)),
-            dma, dma, dma, dma, dma, dma,
+            dma, dma, dma, dma((PARTS,)), dma, dma((PARTS,)),
         ],
         compiler_params=pltpu.CompilerParams(
             collective_id=0, has_side_effects=True, vmem_limit_bytes=56 * 2**20
@@ -419,7 +431,7 @@
     )(
         residual, queries, key_rows, value_rows, out_gate, gate_logits,
         head_gain.reshape(1, 128), out_weight, norm_gain.reshape(1, WIDTH),
-        routes, group_score.reshape(1, ROWS), expert_score, gate_weight, up_weight, down_weight,
+        routes.T, group_score.reshape(1, ROWS), expert_score.T, gate_weight, up_weight, down_weight,
     )
 
 

time: 97.8 us -> 68.2 us (0.70)
  Pallas kernels: 92.8 us -> 66.1 us
  local copies, waits for them, and re-layouts: 4.7 us -> 1.88 us
    pallas_call x1, Pallas kernels: 92.8 us -> 66.1 us  [local(): pl.pallas_call(kernel, out_shape=jax.ShapeDtypeStruct((ROWS, WIDTH), BF16...]
    unnamed x3 -> x1, local copies, waits for them, and re-layouts: 4.7 us -> 1.88 us
where the time goes in v2:
time: 68.2 us; the launch traced here: 68 us
  Pallas kernels  66.1 us (97%)
  local copies, waits for them, and re-layouts  1.88 us (3%)
    pallas_call x1, Pallas kernels, local(): pl.pallas_call(kernel, out_shape=jax.ShapeDtypeStruct((ROWS, WIDTH), BF16...  66.1 us
    unnamed x1, local copies, waits for them, and re-layouts  1.88 us

profile of v2, /device:TPU:1, one launch (start us, length us, event | category | flops | bytes accessed | tf_op | source)
XLA Modules:
  0.0 68.0 jit_solution(10928006640603482512)
XLA Ops:
  0.0 66.1 %shard_map.145 = bf16[128,2048]{1,0:T(8,128)(2,1)} custom-call(bf16[128,2048]{1,0:T(8,128)(2,1)} %residual.1, bf16[256,256]{1,0:T(8,128)(2,1)} %queries.1, bf16[256,256]{1,0:T(8,128)(2,1)} %keys.1, bf16[256,512]{1,0:T(8,128)(2,1)} %values.1, bf16[256,512]{1,0:T(8,128)(2,1)} %out_gate.1, bf16[256,256]{1,0:T(8,128)(2,1)} %gate_logits.1, f32[1,128]{1,0:T(1,128)} %bitcast.8, ...), custom_call_target="tpu_custom_call" | custom-call | tf_op jit(solution)/shard_map/pallas_call | solution.py:389
  66.1 1.9 %copy.17 = bf16[128,2048]{1,0:T(8,128)(2,1)} copy(bf16[128,2048]{1,0:T(8,128)(2,1)} %shard_map.145) | data formatting | bytes 1048576

commit v3 on v2

--- a/solution.py
+++ b/solution.py
@@ -49,13 +49,14 @@
 
 
 def kernel(
-    residual, queries, keys, values, out_gate, gate_logits, head_gain, out_weight, norm_gain,
-    routes, group_score, expert_score, gate_weight, up_weight, down_weight,
+    residual, queries, keys, values, out_gate, gate_logits, head_gain_h, out_weight, norm_gain_h,
+    routes_h, group_score_h, expert_score_h, gate_weight, up_weight, down_weight,
     out,
+    head_gain, norm_gain, routes, group_score, expert_score,
     q_v, k_v, v_v, og_v, gl_v, res_v, ow_v, gw_v, uw_v, dw_v,
-    f_v, qd_v, att_v, gain_v, mix_v, pair_v, states, decays, pick_v, comb_v,
+    f_v, qd_v, att_v, gain_v, mix_v, pair_v, states, pick_v, comb_v,
     norm_v, acc_v, nat_v, tile_v, send_v, recv_v, inner_v, back_v, ret_v,
-    in_sem, w_sem, s_send, s_recv, d_send, d_recv, p_send, p_recv, x_send, x_recv, y_send, y_recv,
+    in_sem, w_sem, s_send, s_recv, p_send, p_recv, x_send, x_recv, y_send, y_recv,
 ):
     place = [lax.axis_index(axis) for axis in AXES]
     core = place[3]
@@ -83,6 +84,14 @@
         in_sem,
         0,
     )
+    get_small = fetch(
+        (
+            (head_gain_h, head_gain), (norm_gain_h, norm_gain), (routes_h, routes),
+            (group_score_h, group_score), (expert_score_h, expert_score),
+        ),
+        in_sem,
+        6,
+    )
     get_ow, get_gw, get_uw, get_dw = fetch(
         (
             (out_weight, ow_v), (gate_weight.at[0], gw_v), (up_weight.at[0], uw_v),
@@ -111,66 +120,74 @@
 
     lane_low = iota((1, 128), 1) < 64
 
-    def state_after(n):
-        rows = n * BLOCK
-        aged = k_v[0:rows, :].astype(F32) * jnp.exp(end_row(n) - f_v[0:rows, :])
+    def state_after(n, p):
+        rows, lanes = n * BLOCK, slice(p * 128, (p + 1) * 128)
+        aged = k_v[0:rows, lanes].astype(F32) * jnp.exp(end_row(n)[:, lanes] - f_v[0:rows, lanes])
         aged = aged.astype(BF16)
-        pairs = []
-        for p in range(PAIRS):
-            side = [
-                dot(
-                    v_v[0:rows, (2 * p + i) * 128 : (2 * p + i + 1) * 128],
-                    aged[:, p * 128 : (p + 1) * 128],
-                    ((0,), (0,)),
-                )
-                for i in range(2)
-            ]
-            pairs.append(jnp.where(lane_low, side[0], side[1]))
-        return pairs
+        side = [
+            dot(v_v[0:rows, (2 * p + i) * 128 : (2 * p + i + 1) * 128], aged, ((0,), (0,)))
+            for i in range(2)
+        ]
+        return jnp.where(lane_low, side[0], side[1])
+
+    def put_decays(level, p, line):
+        part_row = iota((16, 128), 0)
+        rows = jnp.zeros((16, 128), F32)
+        for i, part in enumerate(split3(line)):
+            rows = jnp.where(part_row == i, part.astype(F32), rows)
+        states[level, 2 * p, place[level], 64:80, :] = rows.astype(BF16)
+
+    def share(level, piece):
+        here = place[level]
+        rows = pl.ds(0, 80 if piece % 2 == 0 else 64)
+        for step in (2, 1, 3):
+            pltpu.make_async_remote_copy(
+                src_ref=states.at[level, piece, here, rows],
+                dst_ref=states.at[level, piece, here, rows],
+                send_sem=s_send.at[level, piece],
+                recv_sem=s_recv.at[level, piece],
+                device_id=shifted(level, step),
+                device_id_type=MESH,
+            ).start()
+
+    def await_share(level, piece):
+        rows = pl.ds(0, 80 if piece % 2 == 0 else 64)
+        three = states.at[level, piece, pl.ds(0, 3), rows]
+        pltpu.make_async_copy(three, three, s_recv.at[level, piece]).wait()
+        pltpu.make_async_copy(three, three, s_send.at[level, piece]).wait()
+
+    def line_decays(level, p):
+        here = place[level]
+        total = jnp.zeros((1, 128), F32)
+        before = total
+        steps = []
+        for j in range(4):
+            before = jnp.where(here == j, total, before)
+            step = jnp.sum(states[level, 2 * p, j, 64:80, :].astype(F32), axis=0, keepdims=True)
+            steps.append(jnp.exp(step))
+            total = total + step
+        return jnp.exp(before), total, steps
+
+    def run_line(level, piece, steps):
+        here = place[level]
+        state = jnp.zeros((64, 128), F32)
+        enter = state
+        for j in range(4):
+            enter = jnp.where(here == j, state, enter)
+            state = state * steps[j] + states[level, piece, j, 0:64, :].astype(F32)
+        return enter, state
 
     get_k.wait()
     get_v.wait()
-    local_end = state_after(SEG // BLOCK)
-    spot = place[2]
     for p in range(PAIRS):
-        states[2, spot, :, p * 128 : (p + 1) * 128] = local_end[p].astype(BF16)
-    decays[2, spot] = jnp.broadcast_to(end_row(SEG // BLOCK), (8, 256))
-    pl.semaphore_wait(barrier, len(friends))
-
-    def share(level):
-        here = place[level]
-        for step in (2, 1, 3):
-            for buf, ss, rs in ((states, s_send, s_recv), (decays, d_send, d_recv)):
-                pltpu.make_async_remote_copy(
-                    src_ref=buf.at[level, here],
-                    dst_ref=buf.at[level, here],
-                    send_sem=ss.at[level],
-                    recv_sem=rs.at[level],
-                    device_id=shifted(level, step),
-                    device_id_type=MESH,
-                ).start()
-
-    def await_share(level):
-        for buf, ss, rs in ((states, s_send, s_recv), (decays, d_send, d_recv)):
-            three = buf.at[level, pl.ds(0, 3)]
-            pltpu.make_async_copy(three, three, rs.at[level]).wait()
-            pltpu.make_async_copy(three, three, ss.at[level]).wait()
-
-    def run_line(level):
-        here = place[level]
-        state = jnp.zeros((128, 256), F32)
-        total = jnp.zeros((1, 256), F32)
-        enter, before = state, total
-        for j in range(4):
-            enter = jnp.where(here == j, state, enter)
-            before = jnp.where(here == j, total, before)
-            step = decays[level, j, 0:1, :]
-            state = state * jnp.exp(step) + states[level, j].astype(F32)
-            total = total + step
-        return enter, before, state, total
-
-    share(2)
-
+        local_end = state_after(SEG // BLOCK, p).astype(BF16)
+        states[2, 2 * p, place[2], 0:64, :] = local_end[0:64]
+        put_decays(2, p, end_row(SEG // BLOCK)[:, p * 128 : (p + 1) * 128])
+        states[2, 2 * p + 1, place[2], 0:64, :] = local_end[64:128]
+        if p == 0:
+            pl.semaphore_wait(barrier, len(friends))
+        share(2, 2 * p)
+        share(2, 2 * p + 1)
     get_q.wait()
     scale = 64.0 ** (-0.5)
     block_row = iota((SEG, 1), 0) // BLOCK
@@ -187,7 +204,7 @@
     causal = (row >= col) & (row // BLOCK == col // BLOCK)
     none = jnp.zeros((), BF16)
     local_states = [None] + [
-        [s.astype(BF16) for s in state_after(n)] for n in range(1, SEG // BLOCK)
+        [state_after(n, p).astype(BF16) for p in range(PAIRS)] for n in range(1, SEG // BLOCK)
     ]
     for h in range(HEADS):
         p = h // 2
@@ -202,6 +219,8 @@
             rows = slice(n * BLOCK, (n + 1) * BLOCK)
             att_v[rows, here] += dot(q_h[rows], local_states[n][p], ((1,), (1,)))
     get_og.wait()
+    for copy in get_small:
+        copy.wait()
     for h in range(HEADS):
         here = slice(h * 128, (h + 1) * 128)
         gain_v[:, here] = silu(og_v[:, here].astype(F32)) * head_gain[...]
@@ -244,50 +263,64 @@
         comb_v[part, 0:ROWS] = mid
         comb_v[part, ROWS : 2 * ROWS] = high
 
-    entering = None
-    scales = []
-    enters = []
-    for level in (2, 1, 0):
-        await_share(level)
-        enter, before, state, total = run_line(level)
-        if level:
-            upper = level - 1
-            states[upper, place[upper]] = state.astype(BF16)
-            decays[upper, place[upper]] = jnp.broadcast_to(total, (8, 256))
-            share(upper)
-        enters.append(enter)
-        scales.append(jnp.exp(before))
-    entering = enters[0] + scales[0] * (enters[1] + scales[1] * enters[2])
-    entering = entering.astype(BF16)
-
-    for h in range(HEADS):
-        p = h // 2
-        mine = lane_low if h % 2 == 0 else jnp.logical_not(lane_low)
-        lanes = slice(p * 128, (p + 1) * 128)
-        here = slice(h * 128, (h + 1) * 128)
-        q_h = jnp.where(mine, qd_v[:, lanes], none)
-        attended = att_v[:, here] + dot(q_h, entering[:, lanes], ((1,), (1,)))
-        mean = jnp.mean(attended * attended, axis=-1, keepdims=True)
-        mix_v[:, here] = (attended * lax.rsqrt(mean + 1e-06) * gain_v[:, here]).astype(BF16)
     other_rows = pl.ds(pl.multiple_of((1 - core) * ROWS, ROWS), ROWS)
     own_rows = pl.ds(pl.multiple_of(core * ROWS, ROWS), ROWS)
-    swap = pltpu.make_async_remote_copy(
-        src_ref=mix_v.at[other_rows],
-        dst_ref=pair_v,
-        send_sem=p_send,
-        recv_sem=p_recv,
-        device_id=shifted(3, 1),
-        device_id_type=MESH,
-    )
-    swap.start()
-    get_res.wait()
-    get_ow.wait()
-    half = HEADS * 128
-    own_w = pl.ds(pl.multiple_of(core * half, half), half)
-    other_w = pl.ds(pl.multiple_of((1 - core) * half, half), half)
-    summed = res_v[...].astype(F32) + dot(mix_v[own_rows, :], ow_v[own_w, :])
-    swap.wait()
-    summed = summed + dot(pair_v[...], ow_v[other_w, :])
+    swaps = [
+        pltpu.make_async_remote_copy(
+            src_ref=mix_v.at[p, other_rows],
+            dst_ref=pair_v.at[p],
+            send_sem=p_send.at[p],
+            recv_sem=p_recv.at[p],
+            device_id=shifted(3, 1),
+            device_id_type=MESH,
+        )
+        for p in range(PAIRS)
+    ]
+
+    def project(mixed, whose, p):
+        first = pl.multiple_of(whose * (HEADS * 128) + p * 256, 256)
+        return dot(mixed, ow_v[pl.ds(first, 256), :])
+
+    entered = [[] for _ in range(2 * PAIRS)]
+    for level in (2, 1, 0):
+        for piece in range(2 * PAIRS):
+            p = piece // 2
+            await_share(level, piece)
+            if piece % 2 == 0:
+                scale, total, steps = line_decays(level, p)
+            enter, state = run_line(level, piece, steps)
+            entered[piece].append((scale, enter))
+            if level:
+                upper = level - 1
+                states[upper, piece, place[upper], 0:64, :] = state.astype(BF16)
+                if piece % 2 == 0:
+                    put_decays(upper, p, total)
+                share(upper, piece)
+            elif piece % 2 == 1:
+                halves = []
+                for past in entered[piece - 1 : piece + 1]:
+                    (scale_x, enter_x), (scale_y, enter_y), (_, enter_z) = past
+                    halves.append(enter_x + scale_x * (enter_y + scale_y * enter_z))
+                entering = jnp.concatenate(halves, axis=0).astype(BF16)
+                for h in (2 * p, 2 * p + 1):
+                    mine = lane_low if h % 2 == 0 else jnp.logical_not(lane_low)
+                    here = slice(h * 128, (h + 1) * 128)
+                    q_h = jnp.where(mine, qd_v[:, p * 128 : (p + 1) * 128], none)
+                    attended = att_v[:, here] + dot(q_h, entering, ((1,), (1,)))
+                    mean = jnp.mean(attended * attended, axis=-1, keepdims=True)
+                    mixed = attended * lax.rsqrt(mean + 1e-06) * gain_v[:, here]
+                    mix_v[p, :, (h % 2) * 128 : (h % 2 + 1) * 128] = mixed.astype(BF16)
+                swaps[p].start()
+                if p == 0:
+                    get_res.wait()
+                    get_ow.wait()
+                    acc_v[...] = res_v[...].astype(F32) + project(mix_v[p, own_rows, :], core, p)
+                else:
+                    acc_v[...] += project(mix_v[p, own_rows, :], core, p)
+    swaps[0].wait()
+    acc_v[...] += project(pair_v[0], 1 - core, 0)
+    swaps[1].wait()
+    summed = acc_v[...] + project(pair_v[1], 1 - core, 1)
     wide = summed.astype(BF16).astype(F32)
     acc_v[...] = wide
     mean = jnp.mean(wide * wide, axis=-1, keepdims=True)
@@ -388,10 +421,15 @@
     dma = pltpu.SemaphoreType.DMA
     return pl.pallas_call(
         kernel,
-        out_shape=jax.ShapeDtypeStruct((ROWS, WIDTH), BF16),
-        in_specs=[anywhere] * 6 + [vmem, anywhere, vmem, vmem, vmem, vmem] + [anywhere] * 3,
+        out_shape=pltpu.VMEM((ROWS, WIDTH), BF16),
+        in_specs=[anywhere] * 15,
         out_specs=vmem,
         scratch_shapes=[
+            pltpu.VMEM((1, 128), F32),
+            pltpu.VMEM((1, WIDTH), F32),
+            pltpu.VMEM((2, ROWS), I32),
+            pltpu.VMEM((1, ROWS), F32),
+            pltpu.VMEM((2, ROWS), F32),
             pltpu.VMEM((SEG, 256), BF16),
             pltpu.VMEM((SEG, 256), BF16),
             pltpu.VMEM((SEG, half), BF16),
@@ -406,10 +444,9 @@
             pltpu.VMEM((SEG, 256), BF16),
             pltpu.VMEM((SEG, half), F32),
             pltpu.VMEM((SEG, half), F32),
-            pltpu.VMEM((SEG, half), BF16),
-            pltpu.VMEM((ROWS, half), BF16),
-            pltpu.VMEM((3, 4, 128, 256), BF16),
-            pltpu.VMEM((3, 4, 8, 256), F32),
+            pltpu.VMEM((PAIRS, SEG, 256), BF16),
+            pltpu.VMEM((PAIRS, ROWS, 256), BF16),
+            pltpu.VMEM((3, 2 * PAIRS, 4, 80, 128), BF16),
             pltpu.VMEM((SLOTS, ROWS), BF16),
             pltpu.VMEM((PARTS, 2 * ROWS, PART), BF16),
             pltpu.VMEM((ROWS, WIDTH), BF16),
@@ -421,9 +458,9 @@
             pltpu.VMEM((PART, HIDDEN), BF16),
             tiles,
             tiles,
-            dma((6,)), dma((4,)),
-            dma((3,)), dma((3,)), dma((3,)), dma((3,)),
-            dma, dma, dma, dma((PARTS,)), dma, dma((PARTS,)),
+            dma((11,)), dma((4,)),
+            dma((3, 2 * PAIRS)), dma((3, 2 * PAIRS)),
+            dma((PAIRS,)), dma((PAIRS,)), dma, dma((PARTS,)), dma, dma((PARTS,)),
         ],
         compiler_params=pltpu.CompilerParams(
             collective_id=0, has_side_effects=True, vmem_limit_bytes=56 * 2**20

time: 68.2 us -> 62.2 us (0.912)
  Pallas kernels: 66.1 us -> 61.3 us
  local copies, waits for them, and re-layouts: 1.88 us -> 0.8 us
    pallas_call x1, Pallas kernels: 66.1 us -> 61.3 us  [local(): pl.pallas_call(kernel, out_shape=pltpu.VMEM((ROWS, WIDTH), BF16), in_spec...]
    unnamed x1, local copies, waits for them, and re-layouts: 1.88 us -> 0.8 us
where the time goes in v3:
time: 62.2 us; the launch traced here: 62.1 us
  Pallas kernels  61.3 us (99%)
  local copies, waits for them, and re-layouts  0.8 us (1%)
    pallas_call x1, Pallas kernels, local(): pl.pallas_call(kernel, out_shape=pltpu.VMEM((ROWS, WIDTH), BF16), in_spec...  61.3 us

profile of v3, /device:TPU:1, one launch (start us, length us, event | category | flops | bytes accessed | tf_op | source)
XLA Modules:
  0.0 62.1 jit_solution(6530207266268828236)
XLA Ops:
  0.0 61.3 %shard_map.145 = bf16[128,2048]{1,0:T(8,128)(2,1)S(1)} custom-call(bf16[128,2048]{1,0:T(8,128)(2,1)} %residual.1, bf16[256,256]{1,0:T(8,128)(2,1)} %queries.1, bf16[256,256]{1,0:T(8,128)(2,1)} %keys.1, bf16[256,512]{1,0:T(8,128)(2,1)} %values.1, bf16[256,512]{1,0:T(8,128)(2,1)} %out_gate.1, bf16[256,256]{1,0:T(8,128)(2,1)} %gate_logits.1, f32[1,128]{1,0:T(1,128)} %bitcast.8, ...), custom_call_target="tpu_custom_call" | custom-call | tf_op jit(solution)/shard_map/pallas_call | solution.py:422
  61.3 0.8 %copy.17 = bf16[128,2048]{1,0:T(8,128)(2,1)} copy(bf16[128,2048]{1,0:T(8,128)(2,1)S(1)} %shard_map.145) | data formatting | bytes 1048576

commit v4 on v3

--- a/solution.py
+++ b/solution.py
@@ -16,15 +16,19 @@
 ROWS = 128
 HEADS = 4
 PAIRS = HEADS // 2
+SPLIT = 4
+PIECES = PAIRS * SPLIT
+PIECE = 128 // SPLIT
 WIDTH = 2048
 CHUNKS = WIDTH // 128
 HIDDEN = 512
 DEVICES = 128
 CAP = 3
 SLOTS = DEVICES * CAP
-PARTS = 4
-STEPS = DEVICES // PARTS
-PART = STEPS * CAP
+BOUNDS = (0, 32, 64, 96, 128)
+PARTS = len(BOUNDS) - 1
+SIZES = [(BOUNDS[i + 1] - BOUNDS[i]) * CAP for i in range(PARTS)]
+PART = max(SIZES)
 STRIDE, UNSTRIDE = 53, 29
 PITCH = CHUNKS + 1
 
@@ -38,6 +42,15 @@
     rest = x - high.astype(F32)
     mid = rest.astype(BF16)
     return high, mid, (rest - mid.astype(F32)).astype(BF16)
+
+
+def split2(x):
+    high = x.astype(BF16)
+    return high, (x - high.astype(F32)).astype(BF16)
+
+
+def dot_split(a, b, dims=((1,), (0,))):
+    return dot(a[0], b[0], dims) + (dot(a[0], b[1], dims) + dot(a[1], b[0], dims))
 
 
 def iota(shape, dim):
@@ -123,27 +136,29 @@
     def state_after(n, p):
         rows, lanes = n * BLOCK, slice(p * 128, (p + 1) * 128)
         aged = k_v[0:rows, lanes].astype(F32) * jnp.exp(end_row(n)[:, lanes] - f_v[0:rows, lanes])
-        aged = aged.astype(BF16)
-        side = [
-            dot(v_v[0:rows, (2 * p + i) * 128 : (2 * p + i + 1) * 128], aged, ((0,), (0,)))
-            for i in range(2)
-        ]
+        side = []
+        for i in range(2):
+            v_h = v_v[0:rows, (2 * p + i) * 128 : (2 * p + i + 1) * 128]
+            side.append(sum(dot(v_h, part, ((0,), (0,))) for part in split2(aged)))
         return jnp.where(lane_low, side[0], side[1])
 
-    def put_decays(level, p, line):
+    def put_decays(level, lines):
         part_row = iota((16, 128), 0)
         rows = jnp.zeros((16, 128), F32)
-        for i, part in enumerate(split3(line)):
-            rows = jnp.where(part_row == i, part.astype(F32), rows)
-        states[level, 2 * p, place[level], 64:80, :] = rows.astype(BF16)
+        for p in range(PAIRS):
+            for i, part in enumerate(split3(lines[p])):
+                rows = jnp.where(part_row == 3 * p + i, part.astype(F32), rows)
+        states[level, 0, place[level], PIECE : PIECE + 16, :] = rows.astype(BF16)
+
+    def piece_rows(piece):
+        return pl.ds(0, PIECE + 16 if piece == 0 else PIECE)
 
     def share(level, piece):
         here = place[level]
-        rows = pl.ds(0, 80 if piece % 2 == 0 else 64)
         for step in (2, 1, 3):
             pltpu.make_async_remote_copy(
-                src_ref=states.at[level, piece, here, rows],
-                dst_ref=states.at[level, piece, here, rows],
+                src_ref=states.at[level, piece, here, piece_rows(piece)],
+                dst_ref=states.at[level, piece, here, piece_rows(piece)],
                 send_sem=s_send.at[level, piece],
                 recv_sem=s_recv.at[level, piece],
                 device_id=shifted(level, step),
@@ -151,8 +166,7 @@
             ).start()
 
     def await_share(level, piece):
-        rows = pl.ds(0, 80 if piece % 2 == 0 else 64)
-        three = states.at[level, piece, pl.ds(0, 3), rows]
+        three = states.at[level, piece, pl.ds(0, 3), piece_rows(piece)]
         pltpu.make_async_copy(three, three, s_recv.at[level, piece]).wait()
         pltpu.make_async_copy(three, three, s_send.at[level, piece]).wait()
 
@@ -163,31 +177,33 @@
         steps = []
         for j in range(4):
             before = jnp.where(here == j, total, before)
-            step = jnp.sum(states[level, 2 * p, j, 64:80, :].astype(F32), axis=0, keepdims=True)
+            parts = states[level, 0, j, PIECE : PIECE + 16, :].astype(F32)
+            step = (parts[3 * p + 2 : 3 * p + 3] + parts[3 * p + 1 : 3 * p + 2]) + parts[3 * p : 3 * p + 1]
             steps.append(jnp.exp(step))
             total = total + step
         return jnp.exp(before), total, steps
 
     def run_line(level, piece, steps):
         here = place[level]
-        state = jnp.zeros((64, 128), F32)
+        state = jnp.zeros((PIECE, 128), F32)
         enter = state
         for j in range(4):
             enter = jnp.where(here == j, state, enter)
-            state = state * steps[j] + states[level, piece, j, 0:64, :].astype(F32)
+            state = state * steps[j] + states[level, piece, j, 0:PIECE, :].astype(F32)
         return enter, state
 
     get_k.wait()
     get_v.wait()
+    whole = end_row(SEG // BLOCK)
+    put_decays(2, [whole[:, p * 128 : (p + 1) * 128] for p in range(PAIRS)])
     for p in range(PAIRS):
         local_end = state_after(SEG // BLOCK, p).astype(BF16)
-        states[2, 2 * p, place[2], 0:64, :] = local_end[0:64]
-        put_decays(2, p, end_row(SEG // BLOCK)[:, p * 128 : (p + 1) * 128])
-        states[2, 2 * p + 1, place[2], 0:64, :] = local_end[64:128]
+        for i in range(SPLIT):
+            states[2, p * SPLIT + i, place[2], 0:PIECE, :] = local_end[i * PIECE : (i + 1) * PIECE]
         if p == 0:
             pl.semaphore_wait(barrier, len(friends))
-        share(2, 2 * p)
-        share(2, 2 * p + 1)
+        for i in range(SPLIT):
+            share(2, p * SPLIT + i)
     get_q.wait()
     scale = 64.0 ** (-0.5)
     block_row = iota((SEG, 1), 0) // BLOCK
@@ -197,27 +213,29 @@
         start = jnp.where(block_row == n, end_row(n), start)
     running = f - start
     q = q_v[...].astype(F32) * scale
-    qd_v[...] = (q * jnp.exp(f)).astype(BF16)
-    q_scaled = (q * jnp.exp(running)).astype(BF16)
-    k_inverse = (k_v[...].astype(F32) * jnp.exp(-running)).astype(BF16)
+    for i, part in enumerate(split2(q * jnp.exp(f))):
+        qd_v[i] = part
+    q_scaled = split2(q * jnp.exp(running))
+    k_inverse = split2(k_v[...].astype(F32) * jnp.exp(-running))
     row, col = iota((SEG, SEG), 0), iota((SEG, SEG), 1)
     causal = (row >= col) & (row // BLOCK == col // BLOCK)
     none = jnp.zeros((), BF16)
     local_states = [None] + [
-        [state_after(n, p).astype(BF16) for p in range(PAIRS)] for n in range(1, SEG // BLOCK)
+        [split2(state_after(n, p)) for p in range(PAIRS)] for n in range(1, SEG // BLOCK)
     ]
     for h in range(HEADS):
         p = h // 2
         mine = lane_low if h % 2 == 0 else jnp.logical_not(lane_low)
         lanes = slice(p * 128, (p + 1) * 128)
-        q_h = jnp.where(mine, q_scaled[:, lanes], none)
-        k_h = jnp.where(mine, k_inverse[:, lanes], none)
-        scores = jnp.where(causal, dot(q_h, k_h, ((1,), (1,))), 0.0).astype(BF16)
+        q_h = [jnp.where(mine, part[:, lanes], none) for part in q_scaled]
+        k_h = [jnp.where(mine, part[:, lanes], none) for part in k_inverse]
+        scores = jnp.where(causal, dot_split(q_h, k_h, ((1,), (1,))), 0.0)
         here = slice(h * 128, (h + 1) * 128)
-        att_v[:, here] = dot(scores, v_v[:, here])
+        att_v[:, here] = sum(dot(part, v_v[:, here]) for part in split2(scores))
         for n in range(1, SEG // BLOCK):
             rows = slice(n * BLOCK, (n + 1) * BLOCK)
-            att_v[rows, here] += dot(q_h[rows], local_states[n][p], ((1,), (1,)))
+            q_n = [part[rows] for part in q_h]
+            att_v[rows, here] += dot_split(q_n, local_states[n][p], ((1,), (1,)))
     get_og.wait()
     for copy in get_small:
         copy.wait()
@@ -253,15 +271,15 @@
     score = [as_column(expert_score[c : c + 1, :]) for c in range(2)]
     group = as_column(group_score[...])
     slot_columns = [as_column(line) for line in slot_rows]
-    for part in range(PARTS):
-        slot_lane = (iota((ROWS, PART), 1) + part * PART).astype(F32)
-        comb = jnp.zeros((ROWS, PART), F32)
+    for part, size in enumerate(SIZES):
+        slot_lane = (iota((ROWS, size), 1) + BOUNDS[part] * CAP).astype(F32)
+        comb = jnp.zeros((ROWS, size), F32)
         for c in range(2):
             weight = group * score[c] / (score[0] + score[1])
             comb = comb + jnp.where(slot_lane == slot_columns[c], weight, 0.0)
         high, mid, _ = split3(comb)
-        comb_v[part, 0:ROWS] = mid
-        comb_v[part, ROWS : 2 * ROWS] = high
+        comb_v[part, 0:ROWS, 0:size] = mid
+        comb_v[part, ROWS : 2 * ROWS, 0:size] = high
 
     other_rows = pl.ds(pl.multiple_of((1 - core) * ROWS, ROWS), ROWS)
     own_rows = pl.ds(pl.multiple_of(core * ROWS, ROWS), ROWS)
@@ -281,32 +299,35 @@
         first = pl.multiple_of(whose * (HEADS * 128) + p * 256, 256)
         return dot(mixed, ow_v[pl.ds(first, 256), :])
 
-    entered = [[] for _ in range(2 * PAIRS)]
+    entered = [[] for _ in range(PIECES)]
     for level in (2, 1, 0):
-        for piece in range(2 * PAIRS):
-            p = piece // 2
+        for piece in range(PIECES):
+            p = piece // SPLIT
             await_share(level, piece)
-            if piece % 2 == 0:
-                scale, total, steps = line_decays(level, p)
+            if piece == 0:
+                lines = [line_decays(level, pair) for pair in range(PAIRS)]
+            scale, total, steps = lines[p]
             enter, state = run_line(level, piece, steps)
             entered[piece].append((scale, enter))
             if level:
                 upper = level - 1
-                states[upper, piece, place[upper], 0:64, :] = state.astype(BF16)
-                if piece % 2 == 0:
-                    put_decays(upper, p, total)
+                states[upper, piece, place[upper], 0:PIECE, :] = state.astype(BF16)
+                if piece == 0:
+                    put_decays(upper, [line[1] for line in lines])
                 share(upper, piece)
-            elif piece % 2 == 1:
-                halves = []
-                for past in entered[piece - 1 : piece + 1]:
+            elif piece % SPLIT == SPLIT - 1:
+                parts = []
+                for past in entered[piece + 1 - SPLIT : piece + 1]:
                     (scale_x, enter_x), (scale_y, enter_y), (_, enter_z) = past
-                    halves.append(enter_x + scale_x * (enter_y + scale_y * enter_z))
-                entering = jnp.concatenate(halves, axis=0).astype(BF16)
+                    parts.append(enter_x + scale_x * (enter_y + scale_y * enter_z))
+                entering = split2(jnp.concatenate(parts, axis=0))
                 for h in (2 * p, 2 * p + 1):
                     mine = lane_low if h % 2 == 0 else jnp.logical_not(lane_low)
                     here = slice(h * 128, (h + 1) * 128)
-                    q_h = jnp.where(mine, qd_v[:, p * 128 : (p + 1) * 128], none)
-                    attended = att_v[:, here] + dot(q_h, entering, ((1,), (1,)))
+                    q_h = [
+                        jnp.where(mine, qd_v[i, :, p * 128 : (p + 1) * 128], none) for i in range(2)
+                    ]
+                    attended = att_v[:, here] + dot_split(q_h, entering, ((1,), (1,)))
                     mean = jnp.mean(attended * attended, axis=-1, keepdims=True)
                     mixed = attended * lax.rsqrt(mean + 1e-06) * gain_v[:, here]
                     mix_v[p, :, (h % 2) * 128 : (h % 2 + 1) * 128] = mixed.astype(BF16)
@@ -328,24 +349,24 @@
 
     def put_columns(j, block):
         for i in range(2):
-            tile_v[pl.ds(2 * j + i, PART, stride=PITCH), :] = block[:, i * 128 : (i + 1) * 128]
+            tile_v[pl.ds(2 * j + i, block.shape[0], stride=PITCH), :] = block[
+                :, i * 128 : (i + 1) * 128
+            ]
 
     def gather_tiles(dst, part):
-        @pl.loop(0, PART // 16)
+        @pl.loop(0, SIZES[part] // 16)
         def _(g):
             for i in range(16):
                 slot = g * 16 + i
-                dst[part * PART + slot] = tile_v[pl.ds(slot * PITCH, CHUNKS), :].astype(BF16)
+                dst[BOUNDS[part] * CAP + slot] = tile_v[pl.ds(slot * PITCH, CHUNKS), :].astype(BF16)
 
     def to_rows(src, part):
-        @pl.loop(0, PART // 32)
-        def _(g):
-            for i in range(2):
-                rows = pl.ds(pl.multiple_of(g * 32 + i * 16, 16), 16)
-                nat_v[rows, :] = src[pl.ds(part * PART + g * 32 + i * 16, 16)].reshape(16, WIDTH)
+        for g in range(SIZES[part] // 16):
+            rows = src[BOUNDS[part] * CAP + g * 16 : BOUNDS[part] * CAP + (g + 1) * 16]
+            nat_v[g * 16 : (g + 1) * 16, :] = rows.reshape(16, WIDTH)
 
     def send_part(part, src, dst, ss, rs, sign):
-        @pl.loop(max(1, part * STEPS), (part + 1) * STEPS)
+        @pl.loop(max(1, BOUNDS[part]), BOUNDS[part + 1])
         def _(i):
             offset = lax.rem(i * STRIDE, DEVICES)
             steps = (
@@ -369,12 +390,12 @@
             dst[0:CAP] = src[0:CAP]
 
     def await_part(part, dst, rs):
-        count = PART - (CAP if part == 0 else 0)
-        rows = dst.at[pl.ds(part * PART, count)]
+        count = SIZES[part] - (CAP if part == 0 else 0)
+        rows = dst.at[pl.ds(BOUNDS[part] * CAP, count)]
         pltpu.make_async_copy(rows, rows, rs.at[part]).wait()
 
     for part in range(PARTS):
-        chosen = pick_v[part * PART : (part + 1) * PART, :]
+        chosen = pick_v[BOUNDS[part] * CAP : BOUNDS[part + 1] * CAP, :]
         for j in range(WIDTH // 256):
             put_columns(j, dot(chosen, norm_v[:, j * 256 : (j + 1) * 256]))
         gather_tiles(send_v, part)
@@ -384,22 +405,24 @@
     get_dw.wait()
     for part in range(PARTS):
         await_part(part, recv_v, x_recv)
+        size = SIZES[part]
         to_rows(recv_v, part)
         for n in range(HIDDEN // 256):
             cols = slice(n * 256, (n + 1) * 256)
-            gated = dot(nat_v[...], gw_v[:, cols])
-            lifted = dot(nat_v[...], uw_v[:, cols])
-            inner_v[:, cols] = (silu(gated) * lifted).astype(BF16)
+            gated = dot(nat_v[0:size, :], gw_v[:, cols])
+            lifted = dot(nat_v[0:size, :], uw_v[:, cols])
+            inner_v[0:size, cols] = (silu(gated) * lifted).astype(BF16)
         for j in range(WIDTH // 256):
-            put_columns(j, dot(inner_v[...], dw_v[:, j * 256 : (j + 1) * 256]))
+            put_columns(j, dot(inner_v[0:size, :], dw_v[:, j * 256 : (j + 1) * 256]))
         gather_tiles(back_v, part)
         send_part(part, back_v, ret_v, y_send, y_recv, -1)
     for part in range(PARTS):
         await_part(part, ret_v, y_recv)
+        size = SIZES[part]
         to_rows(ret_v, part)
         for j in range(WIDTH // 256):
             cols = slice(j * 256, (j + 1) * 256)
-            both = dot(comb_v[part], nat_v[:, cols])
+            both = dot(comb_v[part, :, 0:size], nat_v[0:size, cols])
             total = acc_v[:, cols] + (both[0:ROWS] + both[ROWS : 2 * ROWS])
             if part < PARTS - 1:
                 acc_v[:, cols] = total
@@ -441,12 +464,12 @@
             pltpu.VMEM((WIDTH, HIDDEN), BF16),
             pltpu.VMEM((HIDDEN, WIDTH), BF16),
             pltpu.VMEM((SEG, 256), F32),
-            pltpu.VMEM((SEG, 256), BF16),
+            pltpu.VMEM((2, SEG, 256), BF16),
             pltpu.VMEM((SEG, half), F32),
             pltpu.VMEM((SEG, half), F32),
             pltpu.VMEM((PAIRS, SEG, 256), BF16),
             pltpu.VMEM((PAIRS, ROWS, 256), BF16),
-            pltpu.VMEM((3, 2 * PAIRS, 4, 80, 128), BF16),
+            pltpu.VMEM((3, PIECES, 4, PIECE + 16, 128), BF16),
             pltpu.VMEM((SLOTS, ROWS), BF16),
             pltpu.VMEM((PARTS, 2 * ROWS, PART), BF16),
             pltpu.VMEM((ROWS, WIDTH), BF16),
@@ -459,7 +482,7 @@
             tiles,
             tiles,
             dma((11,)), dma((4,)),
-            dma((3, 2 * PAIRS)), dma((3, 2 * PAIRS)),
+            dma((3, PIECES)), dma((3, PIECES)),
             dma((PAIRS,)), dma((PAIRS,)), dma, dma((PARTS,)), dma, dma((PARTS,)),
         ],
         compiler_params=pltpu.CompilerParams(

time: 62.2 us -> 62.3 us (level)
  no operation moved by 1% of the time
where the time goes in v4:
time: 62.3 us; the launch traced here: 62.2 us
  Pallas kernels  61.4 us (99%)
  local copies, waits for them, and re-layouts  0.8 us (1%)
    pallas_call x1, Pallas kernels, local(): pl.pallas_call(kernel, out_shape=pltpu.VMEM((ROWS, WIDTH), BF16), in_spec...  61.4 us

profile of v4, /device:TPU:1, one launch (start us, length us, event | category | flops | bytes accessed | tf_op | source)
XLA Modules:
  0.0 62.2 jit_solution(7628580762634038427)
XLA Ops:
  0.0 61.4 %shard_map.145 = bf16[128,2048]{1,0:T(8,128)(2,1)S(1)} custom-call(bf16[128,2048]{1,0:T(8,128)(2,1)} %residual.1, bf16[256,256]{1,0:T(8,128)(2,1)} %queries.1, bf16[256,256]{1,0:T(8,128)(2,1)} %keys.1, bf16[256,512]{1,0:T(8,128)(2,1)} %values.1, bf16[256,512]{1,0:T(8,128)(2,1)} %out_gate.1, bf16[256,256]{1,0:T(8,128)(2,1)} %gate_logits.1, f32[1,128]{1,0:T(1,128)} %bitcast.8, ...), custom_call_target="tpu_custom_call" | custom-call | tf_op jit(solution)/shard_map/pallas_call | solution.py:445
  61.4 0.8 %copy.17 = bf16[128,2048]{1,0:T(8,128)(2,1)} copy(bf16[128,2048]{1,0:T(8,128)(2,1)S(1)} %shard_map.145) | data formatting | bytes 1048576

commit v5 on v4

--- a/solution.py
+++ b/solution.py
@@ -29,7 +29,7 @@
 PARTS = len(BOUNDS) - 1
 SIZES = [(BOUNDS[i + 1] - BOUNDS[i]) * CAP for i in range(PARTS)]
 PART = max(SIZES)
-STRIDE, UNSTRIDE = 53, 29
+STRIDE, UNSTRIDE = 91, 83
 PITCH = CHUNKS + 1
 
 
@@ -159,7 +159,7 @@
             pltpu.make_async_remote_copy(
                 src_ref=states.at[level, piece, here, piece_rows(piece)],
                 dst_ref=states.at[level, piece, here, piece_rows(piece)],
-                send_sem=s_send.at[level, piece],
+                send_sem=s_send,
                 recv_sem=s_recv.at[level, piece],
                 device_id=shifted(level, step),
                 device_id_type=MESH,
@@ -168,7 +168,6 @@
     def await_share(level, piece):
         three = states.at[level, piece, pl.ds(0, 3), piece_rows(piece)]
         pltpu.make_async_copy(three, three, s_recv.at[level, piece]).wait()
-        pltpu.make_async_copy(three, three, s_send.at[level, piece]).wait()
 
     def line_decays(level, p):
         here = place[level]
@@ -428,6 +427,9 @@
                 acc_v[:, cols] = total
             else:
                 out[:, cols] = total.astype(BF16)
+    tiles = 9 * (128 * PAIRS + 16) // 16
+    rows = send_v.at[pl.ds(0, tiles)]
+    pltpu.make_async_copy(rows, rows, s_send).wait()
     for src, ss in ((send_v, x_send), (back_v, y_send)):
         rows = src.at[pl.ds(0, SLOTS - CAP)]
         pltpu.make_async_copy(rows, rows, ss).wait()
@@ -482,7 +484,7 @@
             tiles,
             tiles,
             dma((11,)), dma((4,)),
-            dma((3, PIECES)), dma((3, PIECES)),
+            dma, dma((3, PIECES)),
             dma((PAIRS,)), dma((PAIRS,)), dma, dma((PARTS,)), dma, dma((PARTS,)),
         ],
         compiler_params=pltpu.CompilerParams(

time: 62.3 us -> 61 us (0.979)
  Pallas kernels: 61.4 us -> 60.1 us
    pallas_call x1, Pallas kernels: 61.4 us -> 60.1 us  [local(): pl.pallas_call(kernel, out_shape=pltpu.VMEM((ROWS, WIDTH), BF16), in_spec...]
where the time goes in v5:
time: 61 us; the launch traced here: 60.9 us
  Pallas kernels  60.1 us (99%)
  local copies, waits for them, and re-layouts  0.8 us (1%)
    pallas_call x1, Pallas kernels, local(): pl.pallas_call(kernel, out_shape=pltpu.VMEM((ROWS, WIDTH), BF16), in_spec...  60.1 us

profile of v5, /device:TPU:1, one launch (start us, length us, event | category | flops | bytes accessed | tf_op | source)
XLA Modules:
  0.0 60.9 jit_solution(18022328248828852646)
XLA Ops:
  0.0 60.1 %shard_map.145 = bf16[128,2048]{1,0:T(8,128)(2,1)S(1)} custom-call(bf16[128,2048]{1,0:T(8,128)(2,1)} %residual.1, bf16[256,256]{1,0:T(8,128)(2,1)} %queries.1, bf16[256,256]{1,0:T(8,128)(2,1)} %keys.1, bf16[256,512]{1,0:T(8,128)(2,1)} %values.1, bf16[256,512]{1,0:T(8,128)(2,1)} %out_gate.1, bf16[256,256]{1,0:T(8,128)(2,1)} %gate_logits.1, f32[1,128]{1,0:T(1,128)} %bitcast.8, ...), custom_call_target="tpu_custom_call" | custom-call | tf_op jit(solution)/shard_map/pallas_call | solution.py:447
  60.1 0.8 %copy.17 = bf16[128,2048]{1,0:T(8,128)(2,1)} copy(bf16[128,2048]{1,0:T(8,128)(2,1)S(1)} %shard_map.145) | data formatting | bytes 1048576

commit v6 on v5

--- a/solution.py
+++ b/solution.py
@@ -341,10 +341,8 @@
     acc_v[...] += project(pair_v[0], 1 - core, 0)
     swaps[1].wait()
     summed = acc_v[...] + project(pair_v[1], 1 - core, 1)
-    wide = summed.astype(BF16).astype(F32)
-    acc_v[...] = wide
-    mean = jnp.mean(wide * wide, axis=-1, keepdims=True)
-    norm_v[...] = (wide * lax.rsqrt(mean + 1e-06) * norm_gain[...]).astype(BF16)
+    merged = summed.astype(BF16)
+    norm_v[...] = merged
 
     def put_columns(j, block):
         for i in range(2):
@@ -399,6 +397,7 @@
             put_columns(j, dot(chosen, norm_v[:, j * 256 : (j + 1) * 256]))
         gather_tiles(send_v, part)
         send_part(part, send_v, recv_v, x_send, x_recv, 1)
+    acc_v[...] = norm_v[...].astype(F32)
     get_gw.wait()
     get_uw.wait()
     get_dw.wait()
@@ -406,6 +405,9 @@
         await_part(part, recv_v, x_recv)
         size = SIZES[part]
         to_rows(recv_v, part)
+        wide = nat_v[0:size, :].astype(F32)
+        mean = jnp.mean(wide * wide, axis=-1, keepdims=True)
+        nat_v[0:size, :] = (wide * lax.rsqrt(mean + 1e-06) * norm_gain[...]).astype(BF16)
         for n in range(HIDDEN // 256):
             cols = slice(n * 256, (n + 1) * 256)
             gated = dot(nat_v[0:size, :], gw_v[:, cols])
@@ -477,7 +479,7 @@
             pltpu.VMEM((ROWS, WIDTH), BF16),
             pltpu.VMEM((ROWS, WIDTH), F32),
             pltpu.VMEM((PART, WIDTH), BF16),
-            pltpu.VMEM((PART * PITCH, 128), F32),
+            pltpu.VMEM(((PART + 2) * PITCH, 128), F32),
             tiles,
             tiles,
             pltpu.VMEM((PART, HIDDEN), BF16),

time: 61 us -> 60.7 us (level)
  no operation moved by 1% of the time
where the time goes in v6:
time: 60.7 us
  Pallas kernels  59.8 us (99%)
  local copies, waits for them, and re-layouts  0.8 us (1%)
    pallas_call x1, Pallas kernels, local(): pl.pallas_call(kernel, out_shape=pltpu.VMEM((ROWS, WIDTH), BF16), in_spec...  59.8 us

profile of v6, /device:TPU:1, one launch (start us, length us, event | category | flops | bytes accessed | tf_op | source)
XLA Modules:
  0.0 60.7 jit_solution(6435275480468197467)
XLA Ops:
  0.0 59.8 %shard_map.145 = bf16[128,2048]{1,0:T(8,128)(2,1)S(1)} custom-call(bf16[128,2048]{1,0:T(8,128)(2,1)} %residual.1, bf16[256,256]{1,0:T(8,128)(2,1)} %queries.1, bf16[256,256]{1,0:T(8,128)(2,1)} %keys.1, bf16[256,512]{1,0:T(8,128)(2,1)} %values.1, bf16[256,512]{1,0:T(8,128)(2,1)} %out_gate.1, bf16[256,256]{1,0:T(8,128)(2,1)} %gate_logits.1, f32[1,128]{1,0:T(1,128)} %bitcast.8, ...), custom_call_target="tpu_custom_call" | custom-call | tf_op jit(solution)/shard_map/pallas_call | solution.py:449
  59.9 0.8 %copy.17 = bf16[128,2048]{1,0:T(8,128)(2,1)} copy(bf16[128,2048]{1,0:T(8,128)(2,1)S(1)} %shard_map.145) | data formatting | bytes 1048576

commit v7 on v6

--- a/solution.py
+++ b/solution.py
@@ -25,7 +25,7 @@
 DEVICES = 128
 CAP = 3
 SLOTS = DEVICES * CAP
-BOUNDS = (0, 32, 64, 96, 128)
+BOUNDS = (0, 48, 96, 128)
 PARTS = len(BOUNDS) - 1
 SIZES = [(BOUNDS[i + 1] - BOUNDS[i]) * CAP for i in range(PARTS)]
 PART = max(SIZES)

time: 60.7 us -> 60.8 us (level)
  no operation moved by 1% of the time
where the time goes in v7:
time: 60.8 us; the launch traced here: 60.7 us
  Pallas kernels  59.9 us (99%)
  local copies, waits for them, and re-layouts  0.8 us (1%)
    pallas_call x1, Pallas kernels, local(): pl.pallas_call(kernel, out_shape=pltpu.VMEM((ROWS, WIDTH), BF16), in_spec...  59.9 us

profile of v7, /device:TPU:1, one launch (start us, length us, event | category | flops | bytes accessed | tf_op | source)
XLA Modules:
  0.0 60.7 jit_solution(3514905985659745367)
XLA Ops:
  0.0 59.9 %shard_map.145 = bf16[128,2048]{1,0:T(8,128)(2,1)S(1)} custom-call(bf16[128,2048]{1,0:T(8,128)(2,1)} %residual.1, bf16[256,256]{1,0:T(8,128)(2,1)} %queries.1, bf16[256,256]{1,0:T(8,128)(2,1)} %keys.1, bf16[256,512]{1,0:T(8,128)(2,1)} %values.1, bf16[256,512]{1,0:T(8,128)(2,1)} %out_gate.1, bf16[256,256]{1,0:T(8,128)(2,1)} %gate_logits.1, f32[1,128]{1,0:T(1,128)} %bitcast.8, ...), custom_call_target="tpu_custom_call" | custom-call | tf_op jit(solution)/shard_map/pallas_call | solution.py:449
  59.9 0.8 %copy.17 = bf16[128,2048]{1,0:T(8,128)(2,1)} copy(bf16[128,2048]{1,0:T(8,128)(2,1)S(1)} %shard_map.145) | data formatting | bytes 1048576
